TPU v7x, 32 devices: a whole 2x2x4 slice. The times are simulated.
32 devices in a mesh: kv: 8 (over z, y), tp: 4 (over x, core).
Axes of the slice: x: 2, y: 2, z: 4, core: 2. Of those that a mesh axis runs over, the one named last changes fastest.
Arguments:
- hidden_rows: bfloat16 [8192, 4096], P(('kv', 'tp')), may hold values from -6 to 6
- queries: bfloat16 [8192, 4096], P('kv', 'tp'), may hold values from -6 to 6
- key_rows: bfloat16 [8192, 1024], P('kv', 'tp'), may hold values from -6 to 6
- value_rows: bfloat16 [8192, 1024], P('kv', 'tp'), may hold values from -6 to 6
- branch_gates: float32 [2, 32, 8192], P(None, 'tp', 'kv'), may hold values from 0.05 to 0.95
- log_sums: float32 [2, 32, 8192], P(None, 'tp', 'kv'), may hold values from 1 to 7
- chosen: int32 [8, 64, 16], P('tp', 'kv'), may hold values from 0 to 255, as said below
- out_grad: bfloat16 [8192, 4096], P('kv', 'tp'), may hold values from -6 to 6
Outputs:
- grad_queries: bfloat16 [8192, 4096], P('kv', 'tp')
- grad_keys: bfloat16 [8192, 1024], P('kv', 'tp')
- grad_values: bfloat16 [8192, 1024], P('kv', 'tp')
- grad_weight: float32 [4096, 4096], P('kv', 'tp')
Inputs may be any that keep to these rules, and one draw needn't show every extreme that they name: `chosen`: each list names distinct key blocks, among them the blocks that cover the query block's own rows; blocks past a query's position may be named and carry no weight for it. For one key head, the lists of the query blocks of one index of kv name at most 16 key blocks (counted with repetition) that lie at any one other index of kv.
All inputs are finite; a program needn't handle non-finite values.
Results may differ from a plain program's by a relative error of at most 0.011.
Values may be sent and summed in bfloat16 or wider, within the bound.
A program may use at most 128 MiB of HBM per device.

v0:
```python
import functools

import jax
import jax.numpy as jnp
from jax import lax
from jax.experimental import pallas as pl
from jax.experimental.pallas import tpu as pltpu
from jax.sharding import PartitionSpec as P

HEADS = 32
KV_HEADS = 8
HEAD_DIM = 128
QUERY_BLOCK = 128
KEY_BLOCK = 32
POOL_BLOCK = 32
CHOSEN = 16
CAP = 16

F32 = jnp.float32
BF16 = jnp.bfloat16


def dot_nt(a, b):
    return lax.dot_general(a, b, (((1,), (1,)), ((), ())), preferred_element_type=F32)


def dot_nn(a, b):
    return lax.dot_general(a, b, (((1,), (0,)), ((), ())), preferred_element_type=F32)


def branch_back(keys, values, query_stack, cot_stack, log_row, mask, scale):
    scores = dot_nt(keys, query_stack) * scale
    weights = jnp.where(mask, jnp.exp(scores - log_row), 0.0)
    weights_low = weights.astype(BF16)
    grad_prob = dot_nt(values, cot_stack)
    delta = jnp.sum(weights_low.astype(F32) * grad_prob, axis=0, keepdims=True)
    dscore = (weights * (grad_prob - delta)).astype(BF16)
    dquery = dot_nn(keys.T, dscore)
    return dquery, dot_nn(dscore, query_stack) * scale, dot_nn(weights_low, cot_stack)


def attend_kernel(
    group, section, kv_count, scale,
    place_ref, lists_ref, slot_ref, own_ref,
    q_ref, g_ref, gate_ref, log_ref, k_ref, v_ref,
    dq_ref, send_ref, kept_ref,
    pooled_k, pooled_v, pool_dk, pool_dv, kept,
):
    head = pl.program_id(0)
    step = pl.program_id(1)
    pool_count = pooled_k.shape[0]
    tokens = kept_ref.shape[0]
    pool_here = pool_count // kv_count
    chunk = 8 * POOL_BLOCK

    @pl.when(step == 0)
    def _():
        send_ref[...] = jnp.zeros_like(send_ref)
        kept[...] = jnp.zeros_like(kept)
        pool_dk[...] = jnp.zeros_like(pool_dk)
        pool_dv[...] = jnp.zeros_like(pool_dv)
        pick = (
            lax.broadcasted_iota(jnp.int32, (16, 2 * chunk), 1) // POOL_BLOCK
            == lax.broadcasted_iota(jnp.int32, (16, 2 * chunk), 0)
        ).astype(BF16)

        def pool(i, carry):
            rows = pl.ds(pl.multiple_of(i * 2 * chunk, 2 * chunk), 2 * chunk)
            dest = pl.ds(pl.multiple_of(i * 16, 16), 16)
            pooled_k[dest, :] = (dot_nn(pick, k_ref[rows, :]) / POOL_BLOCK).astype(BF16)
            pooled_v[dest, :] = (dot_nn(pick, v_ref[rows, :]) / POOL_BLOCK).astype(BF16)
            return carry

        lax.fori_loop(0, pool_count // 16, pool, 0)

    query_stack = jnp.concatenate(
        [q_ref[:, r * HEAD_DIM : (r + 1) * HEAD_DIM] for r in range(group)], axis=0
    )
    gates = gate_ref[0].T
    grads = [g_ref[:, r * HEAD_DIM : (r + 1) * HEAD_DIM].astype(F32) for r in range(group)]

    def gated(branch):
        cols = [gates[:, branch * group + r : branch * group + r + 1] for r in range(group)]
        return jnp.concatenate([(c * g).astype(BF16) for c, g in zip(cols, grads)], axis=0)

    def log_row(branch):
        return jnp.concatenate(
            [log_ref[0, branch * group + r : branch * group + r + 1, :] for r in range(group)],
            axis=1,
        )

    width = group * QUERY_BLOCK
    first = place_ref[0] * tokens + step * QUERY_BLOCK
    query_pos = first + lax.broadcasted_iota(jnp.int32, (1, width), 1) % QUERY_BLOCK

    pool_end = (
        lax.broadcasted_iota(jnp.int32, (pool_count, width), 0) * POOL_BLOCK + POOL_BLOCK - 1
    )
    dq_pool, dk, dv = branch_back(
        pooled_k[...], pooled_v[...], query_stack, gated(0), log_row(0),
        pool_end <= query_pos, scale,
    )
    pool_dk[...] += dk
    pool_dv[...] += dv

    ids = [lists_ref[head, step * CHOSEN + c] for c in range(CHOSEN)]
    rows = [pl.ds(pl.multiple_of(i * KEY_BLOCK, KEY_BLOCK), KEY_BLOCK) for i in ids]
    keys = jnp.concatenate([k_ref[r, :] for r in rows], axis=0)
    values = jnp.concatenate([v_ref[r, :] for r in rows], axis=0)
    offset = lax.broadcasted_iota(jnp.int32, (KEY_BLOCK, width), 0)
    key_pos = jnp.concatenate([offset + i * KEY_BLOCK for i in ids], axis=0)
    dq_pick, dk, dv = branch_back(
        keys, values, query_stack, gated(1), log_row(1), key_pos <= query_pos, scale
    )
    both = jnp.concatenate([dk, dv], axis=1)
    for c in range(CHOSEN):
        part = both[c * KEY_BLOCK : (c + 1) * KEY_BLOCK]
        slot = pl.multiple_of(slot_ref[head, step * CHOSEN + c], KEY_BLOCK)
        own = pl.multiple_of(own_ref[head, step * CHOSEN + c], KEY_BLOCK)
        send_ref[pl.ds(slot, KEY_BLOCK), :] = part.astype(BF16)
        kept[pl.ds(own, KEY_BLOCK), :] += part

    dq = (dq_pool + dq_pick) * scale
    for r in range(group):
        dq_ref[:, r * HEAD_DIM : (r + 1) * HEAD_DIM] = dq[
            :, r * QUERY_BLOCK : (r + 1) * QUERY_BLOCK
        ].T.astype(BF16)

    @pl.when(step == pl.num_programs(1) - 1)
    def _():
        kept_ref[...] = kept[:tokens, :]
        for owner in range(kv_count):
            at = owner * section + CAP * KEY_BLOCK
            here = slice(owner * pool_here, (owner + 1) * pool_here)
            send_ref[at : at + pool_here, :HEAD_DIM] = pool_dk[here, :].astype(BF16)
            send_ref[at : at + pool_here, HEAD_DIM:] = pool_dv[here, :].astype(BF16)


def settle_kernel(section, kv_count, place_ref, asked_ref, got_ref, kept_ref, gk_ref, gv_ref, acc):
    head = pl.program_id(0)
    tokens = kept_ref.shape[0]
    pool_here = tokens // POOL_BLOCK
    at = CAP * KEY_BLOCK
    pooled = sum(
        got_ref[i * section + at : i * section + at + pool_here, :].astype(F32)
        for i in range(kv_count)
    ) / POOL_BLOCK
    for j in range(pool_here):
        rows = slice(j * POOL_BLOCK, (j + 1) * POOL_BLOCK)
        acc[rows, :] = kept_ref[rows, :] + pooled[j : j + 1, :]

    def source(i, carry):
        other = lax.rem(place_ref[0] + 1 + i, kv_count)
        for c in range(CAP):
            block = asked_ref[head, other * CAP + c]
            rows = pl.ds(pl.multiple_of(block * KEY_BLOCK, KEY_BLOCK), KEY_BLOCK)
            came = pl.ds(pl.multiple_of(other * section + c * KEY_BLOCK, KEY_BLOCK), KEY_BLOCK)
            acc[rows, :] += got_ref[came, :].astype(F32)
        return carry

    lax.fori_loop(0, kv_count - 1, source, 0)
    gk_ref[...] = acc[:, :HEAD_DIM].astype(BF16)
    gv_ref[...] = acc[:, HEAD_DIM:].astype(BF16)


def body(hidden_rows, queries, key_rows, value_rows, branch_gates, log_sums, chosen, out_grad):
    kv_count = lax.axis_size("kv")
    kv_index = lax.axis_index("kv")
    tokens = queries.shape[0]
    kv_local = key_rows.shape[1] // HEAD_DIM
    group = HEADS // KV_HEADS
    scale = HEAD_DIM ** (-0.5)
    seq_len = tokens * kv_count
    steps = tokens // QUERY_BLOCK
    blocks_here = tokens // KEY_BLOCK
    pool_count = seq_len // POOL_BLOCK
    pool_here = tokens // POOL_BLOCK
    request_count = steps * CHOSEN
    section = CAP * KEY_BLOCK + pool_here
    slot_count = kv_count * CAP

    pair_rows = jnp.concatenate([key_rows, value_rows], axis=1)
    every_pair = lax.all_gather(pair_rows, "kv", axis=0, tiled=True)

    lists = chosen.reshape(kv_local, request_count)
    owners = lists // blocks_here
    local_block = lists % blocks_here
    remote = owners != kv_index
    order = jnp.arange(request_count, dtype=jnp.int32)
    rank_in = jnp.sum(
        (
            (owners[:, :, None] == owners[:, None, :]) & (order[None, None, :] < order[None, :, None])
        ).astype(jnp.int32),
        axis=-1,
    )
    slot_index = jnp.where(remote, owners * CAP + rank_in, slot_count)
    wanted = jnp.sum(
        jnp.where(
            slot_index[:, None, :] == jnp.arange(slot_count, dtype=jnp.int32)[None, :, None],
            local_block[:, None, :],
            0,
        ),
        axis=-1,
    )
    asked_for = lax.all_to_all(wanted, "kv", split_axis=1, concat_axis=1, tiled=True)
    slot_row = jnp.where(remote, owners * section + rank_in * KEY_BLOCK, kv_index * section)
    own_row = jnp.where(remote, tokens, local_block * KEY_BLOCK)
    place = kv_index.astype(jnp.int32).reshape(1)

    def per_head(array):
        return (
            array.reshape(2, kv_local, group, tokens)
            .transpose(1, 0, 2, 3)
            .reshape(kv_local, 2 * group, tokens)
        )

    pairs_flops = 2 * kv_local * group * tokens * HEAD_DIM * (pool_count + CHOSEN * KEY_BLOCK) * 5
    wide = 2 * HEAD_DIM
    grad_queries, send, kept = pl.pallas_call(
        functools.partial(attend_kernel, group, section, kv_count, scale),
        grid_spec=pltpu.PrefetchScalarGridSpec(
            num_scalar_prefetch=4,
            grid=(kv_local, steps),
            in_specs=[
                pl.BlockSpec((QUERY_BLOCK, group * HEAD_DIM), lambda h, b, *_: (b, h)),
                pl.BlockSpec((QUERY_BLOCK, group * HEAD_DIM), lambda h, b, *_: (b, h)),
                pl.BlockSpec((1, 2 * group, QUERY_BLOCK), lambda h, b, *_: (h, 0, b)),
                pl.BlockSpec((1, 2 * group, QUERY_BLOCK), lambda h, b, *_: (h, 0, b)),
                pl.BlockSpec((seq_len, HEAD_DIM), lambda h, b, *_: (0, h)),
                pl.BlockSpec((seq_len, HEAD_DIM), lambda h, b, *_: (0, kv_local + h)),
            ],
            out_specs=[
                pl.BlockSpec((QUERY_BLOCK, group * HEAD_DIM), lambda h, b, *_: (b, h)),
                pl.BlockSpec((kv_count * section, wide), lambda h, b, *_: (0, h)),
                pl.BlockSpec((tokens, wide), lambda h, b, *_: (0, h)),
            ],
            scratch_shapes=[
                pltpu.VMEM((pool_count, HEAD_DIM), BF16),
                pltpu.VMEM((pool_count, HEAD_DIM), BF16),
                pltpu.VMEM((pool_count, HEAD_DIM), F32),
                pltpu.VMEM((pool_count, HEAD_DIM), F32),
                pltpu.VMEM((tokens + KEY_BLOCK, wide), F32),
            ],
        ),
        out_shape=[
            jax.ShapeDtypeStruct((tokens, kv_local * group * HEAD_DIM), BF16),
            jax.ShapeDtypeStruct((kv_count * section, kv_local * wide), BF16),
            jax.ShapeDtypeStruct((tokens, kv_local * wide), F32),
        ],
        cost_estimate=pl.CostEstimate(
            flops=pairs_flops, bytes_accessed=24 * 2**20, transcendentals=0
        ),
        name="attend_back",
    )(
        place, lists, slot_row, own_row,
        queries, out_grad, per_head(branch_gates), per_head(log_sums), every_pair, every_pair,
    )

    got = lax.all_to_all(send, "kv", split_axis=0, concat_axis=0, tiled=True)

    hidden_late, _ = lax.optimization_barrier((hidden_rows, every_pair))
    whole_rows = lax.all_gather(hidden_late, "tp", axis=0, tiled=True)
    terms = lax.dot_general(
        whole_rows, grad_queries, (((0,), (0,)), ((), ())), preferred_element_type=F32
    ).astype(BF16)
    grad_weight = lax.psum_scatter(terms, "kv", scatter_dimension=0, tiled=True).astype(F32)

    grad_keys, grad_values = pl.pallas_call(
        functools.partial(settle_kernel, section, kv_count),
        grid_spec=pltpu.PrefetchScalarGridSpec(
            num_scalar_prefetch=2,
            grid=(kv_local,),
            in_specs=[
                pl.BlockSpec((kv_count * section, wide), lambda h, *_: (0, h)),
                pl.BlockSpec((tokens, wide), lambda h, *_: (0, h)),
            ],
            out_specs=[
                pl.BlockSpec((tokens, HEAD_DIM), lambda h, *_: (0, h)),
                pl.BlockSpec((tokens, HEAD_DIM), lambda h, *_: (0, h)),
            ],
            scratch_shapes=[pltpu.VMEM((tokens, wide), F32)],
        ),
        out_shape=[
            jax.ShapeDtypeStruct((tokens, kv_local * HEAD_DIM), BF16),
            jax.ShapeDtypeStruct((tokens, kv_local * HEAD_DIM), BF16),
        ],
        cost_estimate=pl.CostEstimate(
            flops=4 * 2**20, bytes_accessed=8 * 2**20, transcendentals=0
        ),
        name="settle",
    )(place, asked_for, got, kept)
    return (grad_queries, grad_keys, grad_values, grad_weight)


def solution(mesh):
    placed = (
        P(("kv", "tp"), None),
        P("kv", "tp"),
        P("kv", "tp"),
        P("kv", "tp"),
        P(None, "tp", "kv"),
        P(None, "tp", "kv"),
        P("tp", "kv", None),
        P("kv", "tp"),
    )
    return jax.shard_map(
        body,
        mesh=mesh,
        in_specs=placed,
        out_specs=(P("kv", "tp"), P("kv", "tp"), P("kv", "tp"), P("kv", "tp")),
        check_vma=False,
    )
```

profile of v0, /device:TPU:0, one launch (start us, length us, event | category | flops | bytes accessed | tf_op | source)
XLA Modules:
  0.0 451.8 jit_solution(16493698235967662099)
XLA Ops:
  7.2 0.0 all-gather.3.cloned.1.call-start
  7.2 2.2 pad_maximum_fusion
  9.5 0.0 copy-start.2
  9.5 0.0 copy-start
  9.5 0.0 all-gather.3.cloned.1.call-update
  9.5 0.0 all-gather.5.cloned.1.call-start
  9.5 128.4 %all-gather.3.cloned.1.call-done.k_ref.v_ref = bf16[8192,512]{1,0:T(8,128)(2,1)} async-done(((bf16[1024,512]{1,0:T(8,128)(2,1)}), bf16[8192,512]{1,0:T(8,128)(2,1)}) %all-gather.3.cloned.1.call-update) | async-done | bytes 8388624 | tf_op jit(solution)/shard_map/all_gather | solution.py:183
  137.9 0.0 all-gather.5.cloned.1.call-update
  137.9 0.0 reduce-scatter.2.cloned.1.call-start
  138.0 0.0 copy-done.2
  138.0 0.1 reshape.138.lists_ref
  138.1 0.0 copy-done
  138.1 0.7 reshape.140.gate_ref
  138.8 0.0 copy-done.1
  138.8 0.7 reshape.142.log_ref
  139.5 0.5 multiply_select_fusion
  140.0 0.2 convert_reduce_fusion
  140.2 0.6 add_select_fusion
  140.8 0.0 copy-done.3
  140.8 43.5 %attend_back.1 = (bf16[1024,1024]{1,0:T(8,128)(2,1)}, bf16[4352,512]{1,0:T(8,128)(2,1)}, f32[1024,512]{1,0:T(8,128)}) custom-call(s32[1]{0:T(128)} %bitcast.place_ref, s32[2,128]{1,0:T(2,128)} %copy-done.3, s32[2,128]{1,0:T(2,128)} %get-tuple-element.20.slot_ref, s32[2,128]{1,0:T(2,128)} %get-tuple-element.16.own_ref, bf16[1024,1024]{1,0:T(8,128)(2,1)} %q_ref.1, ...), custom_call_target="tpu_custom_call" | custom-call | flops 8053063680 | bytes 25165824 | tf_op jit(solution)/shard_map/attend_back/pallas_call | solution.py:219
  184.3 11.6 %all-gather.5.cloned.1.call-done = bf16[1024,4096]{1,0:T(8,128)(2,1)} async-done(((bf16[256,4096]{1,0:T(8,128)(2,1)}), bf16[1024,4096]{1,0:T(8,128)(2,1)}) %all-gather.5.cloned.1.call-update) | async-done | bytes 8388624 | tf_op jit(solution)/shard_map/all_gather | solution.py:262
  195.9 14.9 %convolution_convert_fusion = bf16[4096,1024]{1,0:T(8,128)(2,1)} fusion(bf16[1024,4096]{1,0:T(8,128)(2,1)} %all-gather.5.cloned.1.call-done, bf16[1024,1024]{1,0:T(8,128)(2,1)} %get-tuple-element.6), kind=kOutput, calls=%fused_computation | convolution fusion | flops 8594128896 | bytes 18874368 | tf_op jit(solution)/shard_map/dot_general | solution.py:263
  210.8 0.0 reduce-scatter.2.cloned.1.call-update
  210.9 0.1 select_reduce_fusion
  211.0 0.1 all_to_all.14
  211.1 11.9 %all_to_all.22 = s32[2,8,16]{2,0,1:T(2,128)S(1)} all-to-all(s32[2,8,16]{2,0,1:T(2,128)S(1)} %copy.23), channel_id=1, replica_groups=mesh['kv'=8,'tp'=4] {'kv'}, dimensions={1} | all-to-all | bytes 2048 | tf_op jit(solution)/shard_map/all_to_all | solution.py:205
  223.0 4.6 %all-to-all-start.1 = ((bf16[8,544,512]{2,1,0:T(8,128)(2,1)}), bf16[8,544,512]{2,1,0:T(8,128)(2,1)}, u32[]{:S(2)}, u32[]{:S(2)}) async-start(bf16[8,544,512]{2,1,0:T(8,128)(2,1)} %bitcast.11), calls=%async_computation.1 | async-start | bytes 8912896 | tf_op jit(solution)/shard_map/all_to_all | solution.py:259
  227.6 0.7 all_to_all.16.asked_ref
  228.2 155.9 %all-to-all-done.1 = bf16[8,544,512]{2,1,0:T(8,128)(2,1)} async-done(((bf16[8,544,512]{2,1,0:T(8,128)(2,1)}), bf16[8,544,512]{2,1,0:T(8,128)(2,1)}, u32[]{:S(2)}, u32[]{:S(2)}) %all-to-all-start.1) | async-done | bytes 4456480 | tf_op jit(solution)/shard_map/all_to_all | solution.py:259
  384.2 5.3 %settle.1 = (bf16[1024,256]{1,0:T(8,128)(2,1)}, bf16[1024,256]{1,0:T(8,128)(2,1)}) custom-call(s32[1]{0:T(128)} %bitcast.place_ref, s32[2,128]{1,0:T(2,128)} %all_to_all.16.asked_ref, bf16[4352,512]{1,0:T(8,128)(2,1)} %bitcast.4.got_ref, f32[1024,512]{1,0:T(8,128)} %get-tuple-element.12.kept_ref), custom_call_target="tpu_custom_call" | custom-call | flops 4194304 | bytes 8388608 | tf_op jit(solution)/shard_map/settle/pallas_call | solution.py:268
  389.5 53.0 %reduce-scatter.2.cloned.1.call-done = bf16[512,1024]{1,0:T(8,128)(2,1)} async-done(((bf16[4096,1024]{1,0:T(8,128)(2,1)}), bf16[512,1024]{1,0:T(8,128)(2,1)}) %reduce-scatter.2.cloned.1.call-update) | async-done | bytes 1048592 | tf_op jit(solution)/shard_map/reduce_scatter | solution.py:266
  442.5 2.8 convert_element_type.11
  (9 shorter events, 0.1 us)
Async XLA Ops:
  7.2 130.7 %all-gather.3.cloned.1.call-start = ((), (), s32[]{:S(2)}) async-start(), calls=%async_computation.3 | async-start | bytes 9437184 | tf_op jit(solution)/shard_map/all_gather | solution.py:183
  9.5 128.5 %copy-start.2 = (s32[2,8,16]{2,1,0:T(8,128)S(1)}, s32[2,8,16]{2,1,0:T(8,128)}, u32[]{:S(2)}) copy-start(s32[2,8,16]{2,1,0:T(8,128)} %param.14) | copy-start | bytes 3076
  9.5 128.6 %copy-start = (f32[2,8,1024]{2,1,0:T(8,128)S(1)}, f32[2,8,1024]{2,1,0:T(8,128)}, u32[]{:S(2)}) copy-start(f32[2,8,1024]{2,1,0:T(8,128)} %param.12) | copy-start | bytes 196612
  9.5 129.3 %copy-start.1 = (f32[2,8,1024]{2,1,0:T(8,128)S(1)}, f32[2,8,1024]{2,1,0:T(8,128)}, u32[]{:S(2)}) copy-start(f32[2,8,1024]{2,1,0:T(8,128)} %param.13) | copy-start | bytes 196612
  9.5 186.4 %all-gather.5.cloned.1.call-start = ((), (), s32[]{:S(2)}) async-start(), calls=%async_computation.4 | async-start | bytes 10485760 | tf_op jit(solution)/shard_map/all_gather | solution.py:262
  137.9 304.6 %reduce-scatter.2.cloned.1.call-start = ((), (), s32[]{:S(2)}) async-start(), calls=%async_computation.5 | async-start | bytes 9437184 | tf_op jit(solution)/shard_map/reduce_scatter | solution.py:266
  138.1 2.7 copy-start.3
  223.0 161.2 %all-to-all-start.1 = ((bf16[8,544,512]{2,1,0:T(8,128)(2,1)}), bf16[8,544,512]{2,1,0:T(8,128)(2,1)}, u32[]{:S(2)}, u32[]{:S(2)}) async-start(bf16[8,544,512]{2,1,0:T(8,128)(2,1)} %bitcast.11), calls=%async_computation.1 | async-start | bytes 8912896 | tf_op jit(solution)/shard_map/all_to_all | solution.py:259
Sparse Core Ops, SparseCore 0:
  10.7 127.1 all-gather.2
  139.5 56.4 all-gather.4
  211.0 231.4 reduce-scatter.1
where the time goes:
time: 452 us
  waiting for transfers between devices  349 us (77%)
  Pallas kernels  48.8 us (11%)
  matrix products  14.9 us (3%)
  between operations  13.8 us (3%)
  blocking collectives  11.9 us (3%)
  other arithmetic  6.46 us (1%)
  starting transfers between devices  4.7 us (1%)
    all_to_all x1, waiting for transfers between devices, body(): got = lax.all_to_all(send, 'kv', split_axis=0, concat_axis=0, tiled=True)  156 us
    all_gather x1, waiting for transfers between devices, body(): every_pair = lax.all_gather(pair_rows, 'kv', axis=0, tiled=True)  128 us
    reduce_scatter x1, waiting for transfers between devices, body(): lax.psum_scatter(terms, 'kv', scatter_dimension=0, tiled=True).astype(F32)  53 us
    pallas_call x1, Pallas kernels, body(): pl.pallas_call(functools.partial(attend_kernel, group, section, kv_count,...  43.5 us
    dot_general x1, matrix products, body(): lax.dot_general(whole_rows, grad_queries, (((0,), (0,)), ((), ())), prefe...  14.9 us
    all_to_all x1, blocking collectives, body(): lax.all_to_all(wanted, 'kv', split_axis=1, concat_axis=1, tiled=True)  11.9 us
    all_gather x1, waiting for transfers between devices, body(): whole_rows = lax.all_gather(hidden_late, 'tp', axis=0, tiled=True)  11.6 us
  transfers between devices with their start and end apart: 4, of which 4 were waited for; matrix products, arithmetic and copies ran while one was open for 1% of the time, Pallas kernels for 11%

commit v1 on v0

--- a/solution.py
+++ b/solution.py
@@ -18,6 +18,8 @@
 
 F32 = jnp.float32
 BF16 = jnp.bfloat16
+MESH = pl.DeviceIdType.MESH
+VMEM_LIMIT = 62 * 2**20
 
 
 def dot_nt(a, b):
@@ -136,15 +138,325 @@
             send_ref[at : at + pool_here, HEAD_DIM:] = pool_dv[here, :].astype(BF16)
 
 
-def settle_kernel(section, kv_count, place_ref, asked_ref, got_ref, kept_ref, gk_ref, gv_ref, acc):
+def grid_of(count):
+    width = 1
+    while width * width * 4 <= count:
+        width *= 2
+    while count % width:
+        width //= 2
+    return count // width, width
+
+
+def meet(peers):
+    barrier = pltpu.get_barrier_semaphore()
+    for peer in peers:
+        pl.semaphore_signal(barrier, inc=1, device_id=peer, device_id_type=MESH)
+    pl.semaphore_wait(barrier, len(peers))
+
+
+def gather_kernel(
+    kv_count, tp_count,
+    k_ref, v_ref, hidden_ref, list_ref,
+    k_all, v_all, hidden_all, list_all,
+    z_send, z_recv, y_send, y_recv, h_send, h_recv, l_send, l_recv, own_sem,
+):
+    nz, ny = grid_of(kv_count)
+    me = lax.axis_index("kv")
+    tp = lax.axis_index("tp")
+    z = me // ny
+    y = lax.rem(me, ny)
+    tokens = k_ref.shape[0]
+    hidden_rows = hidden_ref.shape[0]
+    meet(
+        [{"kv": lax.rem(me + d, kv_count)} for d in range(1, kv_count)]
+        + [{"tp": lax.rem(tp + d, tp_count)} for d in range(1, tp_count)]
+    )
+    parts = ((k_ref, k_all), (v_ref, v_all))
+
+    def rows_of(row, col):
+        return pl.ds(pl.multiple_of((row * ny + col) * tokens, tokens), tokens)
+
+    def source(p, s, row):
+        return parts[p][0] if s == 0 else parts[p][1].at[rows_of(row, y)]
+
+    def z_copy(p, side, s, row):
+        to = z + 1 if side == 0 else z - 1
+        return pltpu.make_async_remote_copy(
+            src_ref=source(p, s, row),
+            dst_ref=parts[p][1].at[rows_of(row, y)],
+            send_sem=z_send.at[p, side, s],
+            recv_sem=z_recv.at[p, side, s + 1],
+            device_id={"kv": to * ny + y},
+            device_id_type=MESH,
+        )
+
+    def y_copy(p, side, s, d, row):
+        return pltpu.make_async_remote_copy(
+            src_ref=source(p, s, row),
+            dst_ref=parts[p][1].at[rows_of(row, y)],
+            send_sem=y_send.at[p, side, s, d - 1],
+            recv_sem=y_recv.at[p, side, s, d - 1],
+            device_id={"kv": z * ny + lax.rem(y + d, ny)},
+            device_id_type=MESH,
+        )
+
+    def h_copy(d):
+        at = pl.ds(pl.multiple_of(tp * hidden_rows, hidden_rows), hidden_rows)
+        return pltpu.make_async_remote_copy(
+            src_ref=hidden_ref,
+            dst_ref=hidden_all.at[at],
+            send_sem=h_send.at[d - 1],
+            recv_sem=h_recv.at[d - 1],
+            device_id={"tp": lax.rem(tp + d, tp_count)},
+            device_id_type=MESH,
+        )
+
+    def l_copy(d):
+        return pltpu.make_async_remote_copy(
+            src_ref=list_ref,
+            dst_ref=list_all.at[me],
+            send_sem=l_send.at[d - 1],
+            recv_sem=l_recv.at[d - 1],
+            device_id={"kv": lax.rem(me + d, kv_count)},
+            device_id_type=MESH,
+        )
+
+    def spread(side, s):
+        row = z - s if side == 0 else z + s
+        last = z < nz - 1 if side == 0 else z > 0
+        for p in range(2):
+            @pl.when(last)
+            def _():
+                z_copy(p, side, s, row).start()
+
+            if s > 0 or side == 0:
+                for d in range(1, ny):
+                    y_copy(p, side, s, d, row).start()
+
+    spread(0, 0)
+    spread(1, 0)
+    for d in range(1, tp_count):
+        h_copy(d).start()
+    for d in range(1, kv_count):
+        l_copy(d).start()
+    own = [
+        pltpu.make_async_copy(k_ref, k_all.at[rows_of(z, y)], own_sem.at[0]),
+        pltpu.make_async_copy(v_ref, v_all.at[rows_of(z, y)], own_sem.at[1]),
+        pltpu.make_async_copy(
+            hidden_ref,
+            hidden_all.at[pl.ds(pl.multiple_of(tp * hidden_rows, hidden_rows), hidden_rows)],
+            own_sem.at[2],
+        ),
+        pltpu.make_async_copy(list_ref, list_all.at[me], own_sem.at[3]),
+    ]
+    for copy in own:
+        copy.start()
+
+    def there(side, s):
+        return z >= s if side == 0 else z + s < nz
+
+    for s in range(1, nz):
+        for side in range(2):
+            @pl.when(there(side, s))
+            def _():
+                row = z - s if side == 0 else z + s
+                for p in range(2):
+                    z_copy(p, side, s - 1, row).wait_recv()
+                spread(side, s)
+
+    for s in range(nz):
+        for side in range(2):
+            if s == 0 and side == 1:
+                @pl.when(z > 0)
+                def _():
+                    for p in range(2):
+                        z_copy(p, 1, 0, z).wait_send()
+
+                continue
+
+            @pl.when(there(side, s))
+            def _():
+                row = z - s if side == 0 else z + s
+                last = z < nz - 1 if side == 0 else z > 0
+                for p in range(2):
+                    for d in range(1, ny):
+                        y_copy(p, side, s, d, row).wait()
+
+                    @pl.when(last)
+                    def _():
+                        z_copy(p, side, s, row).wait_send()
+
+    for d in range(1, tp_count):
+        h_copy(d).wait()
+    for d in range(1, kv_count):
+        l_copy(d).wait()
+    for copy in own:
+        copy.wait()
+
+
+def weight_kernel(
+    kv_count, section,
+    hidden_ref, dq_ref, send_ref,
+    gw_ref, got_ref,
+    tile, turned, acc, y_out, y_in, z_out, z_in,
+    tile_sem, ys_sem, yr_sem, zs_sem, zr_sem, as_sem, ar_sem,
+):
+    nz, ny = grid_of(kv_count)
+    me = lax.axis_index("kv")
+    z = me // ny
+    y = lax.rem(me, ny)
+    rows, cols = gw_ref.shape
+    width = min(256, cols)
+    right = nz - 1 - z
+    meet([{"kv": lax.rem(me + d, kv_count)} for d in range(1, kv_count)])
+
+    def owner_row(i):
+        return jnp.where(i < right, nz - 1 - i, i - right)
+
+    def exchange(dz, dy):
+        to = lax.rem(z + dz, nz) * ny + lax.rem(y + dy, ny)
+        n = dz * ny + dy
+        return pltpu.make_async_remote_copy(
+            src_ref=send_ref.at[pl.ds(pl.multiple_of(to * section, 32), section)],
+            dst_ref=got_ref.at[pl.ds(pl.multiple_of(me * section, 32), section)],
+            send_sem=as_sem.at[n],
+            recv_sem=ar_sem.at[n],
+            device_id={"kv": to},
+            device_id_type=MESH,
+        )
+
+    jobs = [(i, d) for i in range(nz) for d in range(1, ny)] + [(i, 0) for i in range(nz)]
+
+    def fetch(n):
+        i, d = jobs[n]
+        owner = owner_row(i) * ny + lax.rem(y + d, ny)
+        at = pl.ds(pl.multiple_of(owner * rows, rows), rows)
+        return pltpu.make_async_copy(hidden_ref.at[:, at], tile.at[n % 2], tile_sem.at[n % 2])
+
+    def ready(n):
+        fetch(n).wait()
+        turned[...] = tile[n % 2].T
+        if n + 1 < len(jobs):
+            fetch(n + 1).start()
+
+    def product(c):
+        at = pl.ds(pl.multiple_of(c * width, width), width)
+        return at, dot_nn(turned[...], dq_ref[:, at])
+
+    def y_copy(i, d):
+        return pltpu.make_async_remote_copy(
+            src_ref=y_out.at[i, d - 1],
+            dst_ref=y_in.at[i, d - 1],
+            send_sem=ys_sem.at[i, d - 1],
+            recv_sem=yr_sem.at[i, d - 1],
+            device_id={"kv": z * ny + lax.rem(y + d, ny)},
+            device_id_type=MESH,
+        )
+
+    def slot(i):
+        return jnp.where(i < right, 0, nz) + owner_row(i)
+
+    def z_copy(i):
+        return pltpu.make_async_remote_copy(
+            src_ref=z_out.at[i],
+            dst_ref=z_in.at[slot(i)],
+            send_sem=zs_sem.at[i],
+            recv_sem=zr_sem.at[slot(i)],
+            device_id={"kv": jnp.where(i < right, z + 1, z - 1) * ny + y},
+            device_id_type=MESH,
+        )
+
+    def z_came(at):
+        return pltpu.make_async_remote_copy(
+            src_ref=z_out.at[0],
+            dst_ref=z_in.at[at],
+            send_sem=zs_sem.at[0],
+            recv_sem=zr_sem.at[at],
+            device_id={"kv": lax.rem(me + ny, kv_count)},
+            device_id_type=MESH,
+        )
+
+    fetch(0).start()
+    for dz in range(1, nz):
+        exchange(dz, 0).start()
+    for n, (i, d) in enumerate(jobs):
+        if d == 0:
+            break
+        ready(n)
+
+        def far(c, carry):
+            at, part = product(c)
+            y_out[i, d - 1, :, at] = part.astype(BF16)
+            return carry
+
+        lax.fori_loop(0, cols // width, far, 0)
+        y_copy(i, d).start()
+    for dy in range(1, ny):
+        for dz in range(nz):
+            exchange(dz, dy).start()
+
+    for i in range(nz):
+        ready(nz * (ny - 1) + i)
+        for d in range(1, ny):
+            y_copy(i, d).wait_recv()
+
+        def near(c, carry):
+            at, part = product(c)
+            for d in range(1, ny):
+                part = part + y_in[i, d - 1, :, at].astype(F32)
+            acc[:, at] = part
+            return carry
+
+        lax.fori_loop(0, cols // width, near, 0)
+        if i < nz - 1:
+            came = jnp.where(i < right, z > 0, z < nz - 1)
+
+            @pl.when(came)
+            def _():
+                z_came(slot(i)).wait_recv()
+                z_out[i] = (acc[...] + z_in[slot(i)].astype(F32)).astype(BF16)
+
+            @pl.when(jnp.logical_not(came))
+            def _():
+                z_out[i] = acc[...].astype(BF16)
+
+            z_copy(i).start()
+
+    @pl.when(z > 0)
+    def _():
+        z_came(z).wait_recv()
+        acc[...] += z_in[z].astype(F32)
+
+    @pl.when(z < nz - 1)
+    def _():
+        z_came(nz + z).wait_recv()
+        acc[...] += z_in[nz + z].astype(F32)
+
+    gw_ref[...] = acc[...]
+    for i in range(nz):
+        for d in range(1, ny):
+            y_copy(i, d).wait_send()
+        if i < nz - 1:
+            z_copy(i).wait_send()
+    for dz in range(nz):
+        for dy in range(ny):
+            if dz or dy:
+                exchange(dz, dy).wait()
+
+
+def settle_kernel(
+    section, kv_count, place_ref, asked_ref, got_ref, own_ref, kept_ref, gk_ref, gv_ref, acc
+):
     head = pl.program_id(0)
     tokens = kept_ref.shape[0]
     pool_here = tokens // POOL_BLOCK
     at = CAP * KEY_BLOCK
-    pooled = sum(
-        got_ref[i * section + at : i * section + at + pool_here, :].astype(F32)
-        for i in range(kv_count)
-    ) / POOL_BLOCK
+    pooled = own_ref[at : at + pool_here, :].astype(F32)
+    for i in range(1, kv_count):
+        other = lax.rem(place_ref[0] + i, kv_count)
+        rows = pl.ds(pl.multiple_of(other * section + at, POOL_BLOCK), pool_here)
+        pooled += got_ref[rows, :].astype(F32)
+    pooled = pooled / POOL_BLOCK
     for j in range(pool_here):
         rows = slice(j * POOL_BLOCK, (j + 1) * POOL_BLOCK)
         acc[rows, :] = kept_ref[rows, :] + pooled[j : j + 1, :]
@@ -179,10 +491,34 @@
     section = CAP * KEY_BLOCK + pool_here
     slot_count = kv_count * CAP
 
-    pair_rows = jnp.concatenate([key_rows, value_rows], axis=1)
-    every_pair = lax.all_gather(pair_rows, "kv", axis=0, tiled=True)
-
     lists = chosen.reshape(kv_local, request_count)
+    tp_count = lax.axis_size("tp")
+    nz, ny = grid_of(kv_count)
+    dma = pltpu.SemaphoreType.DMA
+    anywhere = pl.BlockSpec(memory_space=pl.ANY)
+    inside = pl.BlockSpec(memory_space=pltpu.VMEM)
+    k_all, v_all, hidden_all, list_all = pl.pallas_call(
+        functools.partial(gather_kernel, kv_count, tp_count),
+        in_specs=[inside] * 4,
+        out_specs=[anywhere, anywhere, anywhere, inside],
+        out_shape=[
+            jax.ShapeDtypeStruct((seq_len, key_rows.shape[1]), BF16),
+            jax.ShapeDtypeStruct((seq_len, key_rows.shape[1]), BF16),
+            jax.ShapeDtypeStruct((tokens, hidden_rows.shape[1]), BF16),
+            jax.ShapeDtypeStruct((kv_count, kv_local, request_count), jnp.int32),
+        ],
+        scratch_shapes=[
+            dma((2, 2, nz)), dma((2, 2, nz + 1)),
+            dma((2, 2, nz, max(ny - 1, 1))), dma((2, 2, nz, max(ny - 1, 1))),
+            dma((tp_count - 1,)), dma((tp_count - 1,)),
+            dma((kv_count - 1,)), dma((kv_count - 1,)),
+            dma((4,)),
+        ],
+        compiler_params=pltpu.CompilerParams(
+            collective_id=0, has_side_effects=True, vmem_limit_bytes=VMEM_LIMIT
+        ),
+        name="gather",
+    )(key_rows, value_rows, hidden_rows, lists)
     owners = lists // blocks_here
     local_block = lists % blocks_here
     remote = owners != kv_index
@@ -193,16 +529,20 @@
         ).astype(jnp.int32),
         axis=-1,
     )
-    slot_index = jnp.where(remote, owners * CAP + rank_in, slot_count)
-    wanted = jnp.sum(
+    named = list_all.transpose(1, 0, 2)
+    mine = (named // blocks_here == kv_index).astype(jnp.int32)
+    ahead = jnp.sum(
+        mine[:, :, None, :] * (order[None, None, None, :] < order[None, None, :, None]), axis=-1
+    )
+    asked_for = jnp.sum(
         jnp.where(
-            slot_index[:, None, :] == jnp.arange(slot_count, dtype=jnp.int32)[None, :, None],
-            local_block[:, None, :],
+            (mine[:, :, None, :] > 0)
+            & (ahead[:, :, None, :] == jnp.arange(CAP, dtype=jnp.int32)[None, None, :, None]),
+            named[:, :, None, :] % blocks_here,
             0,
         ),
         axis=-1,
-    )
-    asked_for = lax.all_to_all(wanted, "kv", split_axis=1, concat_axis=1, tiled=True)
+    ).reshape(kv_local, slot_count)
     slot_row = jnp.where(remote, owners * section + rank_in * KEY_BLOCK, kv_index * section)
     own_row = jnp.where(remote, tokens, local_block * KEY_BLOCK)
     place = kv_index.astype(jnp.int32).reshape(1)
@@ -227,7 +567,7 @@
                 pl.BlockSpec((1, 2 * group, QUERY_BLOCK), lambda h, b, *_: (h, 0, b)),
                 pl.BlockSpec((1, 2 * group, QUERY_BLOCK), lambda h, b, *_: (h, 0, b)),
                 pl.BlockSpec((seq_len, HEAD_DIM), lambda h, b, *_: (0, h)),
-                pl.BlockSpec((seq_len, HEAD_DIM), lambda h, b, *_: (0, kv_local + h)),
+                pl.BlockSpec((seq_len, HEAD_DIM), lambda h, b, *_: (0, h)),
             ],
             out_specs=[
                 pl.BlockSpec((QUERY_BLOCK, group * HEAD_DIM), lambda h, b, *_: (b, h)),
@@ -253,17 +593,38 @@
         name="attend_back",
     )(
         place, lists, slot_row, own_row,
-        queries, out_grad, per_head(branch_gates), per_head(log_sums), every_pair, every_pair,
-    )
-
-    got = lax.all_to_all(send, "kv", split_axis=0, concat_axis=0, tiled=True)
-
-    hidden_late, _ = lax.optimization_barrier((hidden_rows, every_pair))
-    whole_rows = lax.all_gather(hidden_late, "tp", axis=0, tiled=True)
-    terms = lax.dot_general(
-        whole_rows, grad_queries, (((0,), (0,)), ((), ())), preferred_element_type=F32
-    ).astype(BF16)
-    grad_weight = lax.psum_scatter(terms, "kv", scatter_dimension=0, tiled=True).astype(F32)
+        queries, out_grad, per_head(branch_gates), per_head(log_sums), k_all, v_all,
+    )
+
+    model = hidden_rows.shape[1]
+    out_rows = model // kv_count
+    out_cols = grad_queries.shape[1]
+    unit = (out_rows, out_cols)
+    far = max(ny - 1, 1)
+    grad_weight, got = pl.pallas_call(
+        functools.partial(weight_kernel, kv_count, section),
+        in_specs=[anywhere, inside, anywhere],
+        out_specs=[inside, anywhere],
+        out_shape=[
+            jax.ShapeDtypeStruct(unit, F32),
+            jax.ShapeDtypeStruct(send.shape, BF16),
+        ],
+        scratch_shapes=[
+            pltpu.VMEM((2, tokens, out_rows), BF16),
+            pltpu.VMEM((out_rows, tokens), BF16),
+            pltpu.VMEM(unit, F32),
+            pltpu.VMEM((nz, far) + unit, BF16),
+            pltpu.VMEM((nz, far) + unit, BF16),
+            pltpu.VMEM((nz,) + unit, BF16),
+            pltpu.VMEM((2 * nz,) + unit, BF16),
+            dma((2,)), dma((nz, far)), dma((nz, far)), dma((nz,)), dma((2 * nz,)),
+            dma((kv_count,)), dma((kv_count,)),
+        ],
+        compiler_params=pltpu.CompilerParams(
+            collective_id=1, has_side_effects=True, vmem_limit_bytes=VMEM_LIMIT
+        ),
+        name="weight",
+    )(hidden_all, grad_queries, send)
 
     grad_keys, grad_values = pl.pallas_call(
         functools.partial(settle_kernel, section, kv_count),
@@ -272,6 +633,7 @@
             grid=(kv_local,),
             in_specs=[
                 pl.BlockSpec((kv_count * section, wide), lambda h, *_: (0, h)),
+                pl.BlockSpec((section, wide), lambda h, place, *_: (place[0], h)),
                 pl.BlockSpec((tokens, wide), lambda h, *_: (0, h)),
             ],
             out_specs=[
@@ -288,7 +650,7 @@
             flops=4 * 2**20, bytes_accessed=8 * 2**20, transcendentals=0
         ),
         name="settle",
-    )(place, asked_for, got, kept)
+    )(place, asked_for, got, send, kept)
     return (grad_queries, grad_keys, grad_values, grad_weight)
 
 

time: 452 us -> 329 us (0.73)
  waiting for transfers between devices: 349 us -> 0 us
  Pallas kernels: 48.8 us -> 319 us
  matrix products: 14.9 us -> 0 us
  between operations: 13.8 us -> 0.73 us
  blocking collectives: 11.9 us -> 0 us
  starting transfers between devices: 4.7 us -> 0 us
    pallas_call x0 -> x2, Pallas kernels: none -> 270 us  [the longest x1 166 us: body(): pl.pallas_call(functools.partial(weight_kernel, kv_count, section), in_sp...]
    all_to_all x1 -> x0, waiting for transfers between devices: 156 us -> none  [body(): got = lax.all_to_all(send, 'kv', split_axis=0, concat_axis=0, tiled=True)]
    all_gather x2 -> x0, waiting for transfers between devices: 140 us -> none  [the longest x1 128 us: body(): every_pair = lax.all_gather(pair_rows, 'kv', axis=0, tiled=True)]
    reduce_scatter x1 -> x0, waiting for transfers between devices: 53 us -> none  [body(): lax.psum_scatter(terms, 'kv', scatter_dimension=0, tiled=True).astype(F32)]
    dot_general x1 -> x0, matrix products: 14.9 us -> none  [body(): lax.dot_general(whole_rows, grad_queries, (((0,), (0,)), ((), ())), prefe...]
    all_to_all x1 -> x0, blocking collectives: 11.9 us -> none  [body(): lax.all_to_all(wanted, 'kv', split_axis=1, concat_axis=1, tiled=True)]
    all_to_all x1 -> x0, starting transfers between devices: 4.58 us -> none  [body(): got = lax.all_to_all(send, 'kv', split_axis=0, concat_axis=0, tiled=True)]
  transfers between devices with their start and end apart: 4 -> 0, of which waited for: 4 -> 0; matrix products, arithmetic and copies ran while one was open for 1% -> 0% of each run, Pallas kernels for 11% -> 0%
where the time goes in v1:
time: 329 us
  Pallas kernels  319 us (97%)
  local copies, waits for them, and re-layouts  5.84 us (2%)
  other arithmetic  3.47 us (1%)
    pallas_call x1, Pallas kernels, body(): pl.pallas_call(functools.partial(weight_kernel, kv_count, section), in_sp...  166 us
    pallas_call x1, Pallas kernels, body(): pl.pallas_call(functools.partial(gather_kernel, kv_count, tp_count), in_s...  104 us
    pallas_call x1, Pallas kernels, body(): pl.pallas_call(functools.partial(attend_kernel, group, section, kv_count,...  43 us

profile of v1, /device:TPU:0, one launch (start us, length us, event | category | flops | bytes accessed | tf_op | source)
XLA Modules:
  0.0 328.9 jit_solution(2573714588208259786)
XLA Ops:
  0.6 0.8 reshape.129.list_ref.lists_ref
  1.4 0.0 copy-start.1
  1.4 0.6 fusion.3
  2.0 0.2 convert_reduce_fusion
  2.2 0.6 add_select_fusion.slot_ref
  2.7 0.9 reshape.130
  3.6 0.7 reshape.131.gate_ref
  4.3 0.9 reshape.132
  5.2 0.7 reshape.133.log_ref
  5.8 0.0 copy-done.1
  5.8 103.8 %gather.1 = (bf16[8192,256]{1,0:T(8,128)(2,1)}, bf16[8192,256]{1,0:T(8,128)(2,1)}, bf16[1024,4096]{1,0:T(8,128)(2,1)}, s32[8,2,128]{2,1,0:T(2,128)}) custom-call(bf16[1024,256]{1,0:T(8,128)(2,1)} %k_ref.1, bf16[1024,256]{1,0:T(8,128)(2,1)} %v_ref.1, bf16[256,4096]{1,0:T(8,128)(2,1)} %hidden_ref.1, s32[2,128]{1,0:T(2,128)} %copy-done.1), custom_call_target="tpu_custom_call" | custom-call | tf_op jit(solution)/shard_map/gather/pallas_call | solution.py:500
  109.6 0.7 and_select_fusion
  110.4 0.7 broadcast_compare_fusion
  111.1 0.3 multiply_reduce_fusion
  111.5 0.3 select_reduce_fusion
  111.8 0.7 reshape.134.asked_ref
  112.5 43.0 %attend_back.1 = (bf16[1024,1024]{1,0:T(8,128)(2,1)}, bf16[4352,512]{1,0:T(8,128)(2,1)}, f32[1024,512]{1,0:T(8,128)}) custom-call(s32[1]{0:T(128)} %bitcast.place_ref, s32[2,128]{1,0:T(2,128)} %copy-done.1, s32[2,128]{1,0:T(2,128)} %add_select_fusion.slot_ref, s32[2,128]{1,0:T(2,128)} %get-tuple-element.28.own_ref, bf16[1024,1024]{1,0:T(8,128)(2,1)} %q_ref.1, ...), custom_call_target="tpu_custom_call" | custom-call | flops 8053063680 | bytes 25165824 | tf_op jit(solution)/shard_map/attend_back/pallas_call | solution.py:559
  155.6 166.4 %weight.1 = (f32[512,1024]{1,0:T(8,128)}, bf16[4352,512]{1,0:T(8,128)(2,1)}) custom-call(bf16[1024,4096]{1,0:T(8,128)(2,1)} %get-tuple-element.19.hidden_ref, bf16[1024,1024]{1,0:T(8,128)(2,1)} %get-tuple-element.34.dq_ref, bf16[4352,512]{1,0:T(8,128)(2,1)} %get-tuple-element.20.send_ref.own_ref), custom_call_target="tpu_custom_call" | custom-call | tf_op jit(solution)/shard_map/weight/pallas_call | solution.py:604
  321.9 0.0 copy-start
  321.9 5.6 %settle.1 = (bf16[1024,256]{1,0:T(8,128)(2,1)}, bf16[1024,256]{1,0:T(8,128)(2,1)}) custom-call(s32[1]{0:T(128)} %bitcast.place_ref, s32[2,128]{1,0:T(2,128)} %reshape.134.asked_ref, bf16[4352,512]{1,0:T(8,128)(2,1)} %get-tuple-element.21.got_ref, bf16[4352,512]{1,0:T(8,128)(2,1)} %get-tuple-element.20.send_ref.own_ref, f32[1024,512]{1,0:T(8,128)} %get-tuple-element.22.kept_ref), custom_call_target="tpu_custom_call" | custom-call | flops 4194304 | bytes 8388608 | tf_op jit(solution)/shard_map/settle/pallas_call | solution.py:629
  327.5 0.0 copy-done
  327.5 1.3 copy.35
  (7 shorter events, 0.1 us)
Async XLA Ops:
  1.4 4.4 %copy-start.1 = (s32[2,128]{1,0:T(2,128)}, s32[2,128]{1,0:T(2,128)S(1)}, u32[]{:S(2)}) copy-start(s32[2,128]{1,0:T(2,128)S(1)} %reshape.129.list_ref.lists_ref) | copy-start | bytes 3076
  321.9 5.6 %copy-start = (f32[512,1024]{1,0:T(8,128)S(1)}, f32[512,1024]{1,0:T(8,128)}, u32[]{:S(2)}) copy-start(f32[512,1024]{1,0:T(8,128)} %get-tuple-element.37) | copy-start | bytes 6291460

commit v2 on v0

v2 whole, which is shorter than its diff:
```python
import functools

import jax
import jax.numpy as jnp
from jax import lax
from jax.experimental import pallas as pl
from jax.experimental.pallas import tpu as pltpu
from jax.sharding import PartitionSpec as P

HEADS = 32
KV_HEADS = 8
HEAD_DIM = 128
QUERY_BLOCK = 128
KEY_BLOCK = 32
POOL_BLOCK = 32
CHOSEN = 16
CAP = 16

F32 = jnp.float32
BF16 = jnp.bfloat16
MESH = pl.DeviceIdType.MESH
VMEM_LIMIT = 62 * 2**20


def dot_nt(a, b):
    return lax.dot_general(a, b, (((1,), (1,)), ((), ())), preferred_element_type=F32)


def dot_nn(a, b):
    return lax.dot_general(a, b, (((1,), (0,)), ((), ())), preferred_element_type=F32)


def branch_back(keys, values, query_stack, cot_stack, log_row, mask, scale):
    scores = dot_nt(keys, query_stack) * scale
    weights = jnp.where(mask, jnp.exp(scores - log_row), 0.0)
    weights_low = weights.astype(BF16)
    grad_prob = dot_nt(values, cot_stack)
    delta = jnp.sum(weights_low.astype(F32) * grad_prob, axis=0, keepdims=True)
    dscore = (weights * (grad_prob - delta)).astype(BF16)
    dquery = dot_nn(keys.T, dscore)
    return dquery, dot_nn(dscore, query_stack) * scale, dot_nn(weights_low, cot_stack)


def grid_of(count):
    width = 1
    while width * width * 4 <= count:
        width *= 2
    while count % width:
        width //= 2
    return count // width, width


def meet(peers):
    barrier = pltpu.get_barrier_semaphore()
    for peer in peers:
        pl.semaphore_signal(barrier, inc=1, device_id=peer, device_id_type=MESH)
    pl.semaphore_wait(barrier, len(peers))


def step_kernel(
    kv_count, tp_count, group, scale,
    lists_ref, slots_ref, own_ref,
    wanted_ref, k_ref, v_ref, hidden_ref, gate_ref, log_ref, q_hbm, g_hbm,
    dq_ref, gw_ref, kept_ref, got_ref, pool_got, asked_ref, hid_all,
    q_buf, g_buf, k_heads, v_heads, pooled, pool_acc, pool_out, dq_pool, dq_far,
    parts, out_box, turned, tile, partial, z_out, z_in,
    in_sem, z_send, z_recv, y_send, y_recv, p_send, p_recv, w_send, w_recv, pg_send, pg_recv,
    hy_send, hy_recv, hx_send, hx_recv, hs_send, hs_recv, dq_send, dq_recv,
    a_send, a_recv, s_send, s_recv,
):
    nz, ny = grid_of(kv_count)
    me = lax.axis_index("kv")
    tp = lax.axis_index("tp")
    z = me // ny
    y = lax.rem(me, ny)
    cores = 2 if tp_count % 2 == 0 else 1
    nx = tp_count // cores
    x = tp // cores
    core = lax.rem(tp, cores)
    blocks_here = k_ref.shape[0]
    tokens = blocks_here * KEY_BLOCK
    heads = k_ref.shape[2] // HEAD_DIM
    steps = tokens // QUERY_BLOCK
    requests = steps * CHOSEN
    pool_count = pooled.shape[0] * pooled.shape[1]
    pool_here = pooled.shape[1]
    hidden_rows = hidden_ref.shape[0]
    rows, cols = gw_ref.shape
    head_cols = group * HEAD_DIM
    wide = 2 * HEAD_DIM
    width = group * QUERY_BLOCK
    box = CAP * KEY_BLOCK
    meet(
        [{"kv": lax.rem(me + d, kv_count)} for d in range(1, kv_count)]
        + [{"tp": lax.rem(tp + d, tp_count)} for d in range(1, tp_count)]
    )
    banks = ((k_ref, k_heads), (v_ref, v_heads))

    def remote(src, dst, send, recv, to):
        return pltpu.make_async_remote_copy(
            src_ref=src, dst_ref=dst, send_sem=send, recv_sem=recv,
            device_id=to, device_id_type=MESH,
        )

    def rows_of(row, col):
        return pl.ds((row * ny + col) * blocks_here, blocks_here)

    def source(h, p, s, row):
        if s == 0:
            return banks[p][0].at[:, :, h * HEAD_DIM : (h + 1) * HEAD_DIM]
        return banks[p][1][h].at[rows_of(row, y)]

    def z_copy(h, p, side, s, row):
        to = z + 1 if side == 0 else z - 1
        return remote(
            source(h, p, s, row), banks[p][1][h].at[rows_of(row, y)],
            z_send.at[h, p, side, s], z_recv.at[h, p, side, s + 1], {"kv": to * ny + y},
        )

    def y_copy(h, p, side, s, d, row, col):
        return remote(
            source(h, p, s, row), banks[p][1][h].at[rows_of(row, col)],
            y_send.at[h, p, side, s, d - 1], y_recv.at[h, p, side, s, d - 1],
            {"kv": z * ny + lax.rem(y + d, ny)},
        )

    def there(side, s):
        return z >= s if side == 0 else z + s < nz

    def onward(side):
        return z < nz - 1 if side == 0 else z > 0

    def place(side, s):
        return z - s if side == 0 else z + s

    def pass_z(h, side, s):
        @pl.when(onward(side))
        def _():
            for p in range(2):
                z_copy(h, p, side, s, place(side, s)).start()

    def pass_y(h, side, s):
        for p in range(2):
            for d in range(1, ny):
                y_copy(h, p, side, s, d, place(side, s), y).start()

    def relay_keys(h, s):
        if h >= heads:
            return
        for side in range(2):
            @pl.when(there(side, s))
            def _():
                for p in range(2):
                    z_copy(h, p, side, s - 1, place(side, s)).wait_recv()
                pass_z(h, side, s)
                pass_y(h, side, s)

    def keys_complete(h):
        for s in range(nz):
            for side in range(1 if s == 0 else 2):
                @pl.when(there(side, s))
                def _():
                    for p in range(2):
                        for d in range(1, ny):
                            y_copy(h, p, side, s, d, place(side, s), y).wait_recv()

    def others(make):
        return [make(d) for d in range(1, kv_count)]

    def spread(src, dst, send, recv):
        def make(d):
            to = lax.rem(me + d, kv_count)
            return remote(src(to), dst.at[me], send.at[d - 1], recv.at[d - 1], {"kv": to})

        return others(make)

    fetches = [
        pltpu.make_async_copy(q_hbm, q_buf, in_sem.at[0]),
        pltpu.make_async_copy(g_hbm, g_buf, in_sem.at[1]),
        pltpu.make_async_copy(wanted_ref.at[me], asked_ref.at[me], in_sem.at[2]),
    ]
    for h in range(heads):
        for p in range(2):
            fetches.append(
                pltpu.make_async_copy(
                    source(h, p, 0, z), banks[p][1][h].at[rows_of(z, y)],
                    in_sem.at[3 + 2 * h + p],
                )
            )
    hid_local = [
        pltpu.make_async_copy(
            hidden_ref.at[:, pl.ds(pl.multiple_of((row * ny + y) * rows, rows), rows)],
            hid_all.at[row, pl.ds(pl.multiple_of((y * tp_count + tp) * hidden_rows, hidden_rows), hidden_rows)],
            in_sem.at[3 + 2 * heads + row],
        )
        for row in range(nz)
    ]

    def hid_rows(col, part):
        at = (col * tp_count + part) * hidden_rows
        return hid_all.at[:, pl.ds(pl.multiple_of(at, hidden_rows), hidden_rows)]

    def hy_copy(d, row):
        to = lax.rem(y + d, ny)
        return remote(
            hidden_ref.at[:, pl.ds(pl.multiple_of((row * ny + to) * rows, rows), rows)],
            hid_all.at[row, pl.ds(pl.multiple_of((y * tp_count + tp) * hidden_rows, hidden_rows), hidden_rows)],
            hy_send.at[d - 1, row], hy_recv.at[d - 1, row], {"kv": z * ny + to},
        )

    def hx_copy(e, d):
        col = lax.rem(y + ny - e, ny)
        to = lax.rem(x + d, nx) * cores + core
        return remote(
            hid_rows(col, tp), hid_rows(col, tp),
            hx_send.at[e, d - 1], hx_recv.at[e, d - 1], {"tp": to},
        )

    def hs_copy(e, d):
        col = lax.rem(y + ny - e, ny)
        part = lax.rem(x + nx - d, nx) * cores + core
        return remote(
            hid_rows(col, part), hid_rows(col, part),
            hs_send.at[e, d], hs_recv.at[e, d], {"tp": x * cores + 1 - core},
        )

    def hidden_out(e):
        for d in range(1, nx):
            hx_copy(e, d).start()
        if cores > 1:
            hs_copy(e, 0).start()

    def hidden_on(e):
        for d in range(1, nx):
            hx_copy(e, d).wait_recv()
            if cores > 1:
                hs_copy(e, d).start()

    def exchange(h, dz, dy):
        to = lax.rem(z + dz, nz) * ny + lax.rem(y + dy, ny)
        n = dz * ny + dy
        return remote(
            out_box.at[to],
            got_ref.at[h, pl.ds(pl.multiple_of(me * box, box), box)],
            a_send.at[h, n], a_recv.at[h, n], {"kv": to},
        )

    def dq_copy(h, d):
        return remote(
            dq_ref.at[:, h * head_cols : (h + 1) * head_cols], dq_far.at[h, d - 1],
            dq_send.at[h, d - 1], dq_recv.at[h, d - 1],
            {"kv": z * ny + lax.rem(y + d, ny)},
        )

    right = nz - 1 - z
    right_first = z * 2 < nz

    def owner_row(i):
        ahead = jnp.where(i < right, nz - 1 - i, i - right)
        back = jnp.where(i < z, i, nz - 1 - (i - z))
        return jnp.where(right_first, ahead, back)

    def goes_right(i):
        return jnp.where(right_first, jnp.where(i < right, 1, 0), jnp.where(i < z, 0, 1)) > 0

    def sum_copy(h, i):
        to = jnp.where(goes_right(i), z + 1, z - 1)
        slot = jnp.where(goes_right(i), owner_row(i) - to, nz - to + owner_row(i))
        return remote(
            z_out.at[h, i], z_in.at[h, slot], s_send.at[h, i], s_recv.at[h, slot],
            {"kv": to * ny + y},
        )

    def sum_came(h, slot):
        return remote(
            z_out.at[h, 0], z_in.at[h, slot], s_send.at[h, 0], s_recv.at[h, slot],
            {"kv": lax.rem(me + ny, kv_count)},
        )

    def in_slot(i):
        return jnp.where(goes_right(i), owner_row(i) - z, nz - z + owner_row(i))

    def has_in(i):
        return jnp.where(goes_right(i), jnp.where(z > 0, 1, 0), jnp.where(z < nz - 1, 1, 0)) > 0

    pick = (
        lax.broadcasted_iota(jnp.int32, (pool_here, tokens), 1) // POOL_BLOCK
        == lax.broadcasted_iota(jnp.int32, (pool_here, tokens), 0)
    ).astype(BF16)
    for p in range(2):
        mean = (dot_nn(pick, banks[p][0][...].reshape(tokens, heads * HEAD_DIM)) / POOL_BLOCK).astype(BF16)
        pooled[me, :, p * heads * HEAD_DIM : (p + 1) * heads * HEAD_DIM] = mean
    pool_sends = spread(lambda to: pooled.at[me], pooled, p_send, p_recv)
    for copy in pool_sends:
        copy.start()
    want_sends = spread(lambda to: wanted_ref.at[to], asked_ref, w_send, w_recv)
    pass_z(0, 0, 0)
    pass_z(0, 1, 0)
    pass_y(0, 0, 0)
    for copy in fetches + hid_local + want_sends:
        copy.start()
    parts[requests] = jnp.zeros((KEY_BLOCK, wide), BF16)
    pool_acc[...] = jnp.zeros_like(pool_acc)
    for copy in hid_local:
        copy.wait()
    hidden_out(0)
    for copy in fetches:
        copy.wait()
    for copy in pool_sends:
        copy.wait_recv()

    def load_step(h, b, branch):
        at = pl.ds(pl.multiple_of(b * QUERY_BLOCK, QUERY_BLOCK), QUERY_BLOCK)
        first = h * head_cols
        stack = jnp.concatenate(
            [q_buf[at, first + r * HEAD_DIM : first + (r + 1) * HEAD_DIM] for r in range(group)],
            axis=0,
        )
        gates = gate_ref[branch, :, at].T
        cots = jnp.concatenate(
            [
                (
                    gates[:, h * group + r : h * group + r + 1]
                    * g_buf[at, first + r * HEAD_DIM : first + (r + 1) * HEAD_DIM].astype(F32)
                ).astype(BF16)
                for r in range(group)
            ],
            axis=0,
        )
        logs = log_ref[branch, :, at]
        log_row = jnp.concatenate(
            [logs[h * group + r : h * group + r + 1, :] for r in range(group)], axis=1
        )
        query_pos = (
            me * tokens + b * QUERY_BLOCK
            + lax.broadcasted_iota(jnp.int32, (1, width), 1) % QUERY_BLOCK
        )
        return at, stack, cots, log_row, query_pos

    def pool_steps(h, low, high):
        def one(b, carry):
            at, stack, cots, log_row, query_pos = load_step(h, b, 0)
            pool_end = (
                lax.broadcasted_iota(jnp.int32, (pool_count, width), 0) * POOL_BLOCK
                + POOL_BLOCK - 1
            )
            first = h * HEAD_DIM
            keys = pooled[:, :, first : first + HEAD_DIM].reshape(pool_count, HEAD_DIM)
            first += heads * HEAD_DIM
            values = pooled[:, :, first : first + HEAD_DIM].reshape(pool_count, HEAD_DIM)
            dq, dk, dv = branch_back(
                keys, values, stack, cots, log_row, pool_end <= query_pos, scale
            )
            dq_pool[h * steps + b] = dq
            pool_acc[h] += jnp.concatenate([dk, dv], axis=1)
            return carry

        lax.fori_loop(low, high, one, 0)

    def pick_steps(h, low, high):
        def one(b, carry):
            at, stack, cots, log_row, query_pos = load_step(h, b, 1)
            ids = [lists_ref[h, b * CHOSEN + c] for c in range(CHOSEN)]
            keys = jnp.concatenate([k_heads[h][i] for i in ids], axis=0)
            values = jnp.concatenate([v_heads[h][i] for i in ids], axis=0)
            offset = lax.broadcasted_iota(jnp.int32, (KEY_BLOCK, width), 0)
            key_pos = jnp.concatenate([offset + i * KEY_BLOCK for i in ids], axis=0)
            dq, dk, dv = branch_back(
                keys, values, stack, cots, log_row, key_pos <= query_pos, scale
            )
            parts[pl.ds(b * CHOSEN, CHOSEN)] = (
                jnp.concatenate([dk, dv], axis=1).astype(BF16).reshape(CHOSEN, KEY_BLOCK, wide)
            )
            dq = (dq + dq_pool[h * steps + b]) * scale
            for r in range(group):
                first = h * head_cols + r * HEAD_DIM
                dq_ref[at, first : first + HEAD_DIM] = dq[
                    :, r * QUERY_BLOCK : (r + 1) * QUERY_BLOCK
                ].T.astype(BF16)
            return carry

        lax.fori_loop(low, high, one, 0)

    def pack(h):
        def to_owner(d, carry):
            owner = lax.rem(me + d, kv_count)
            for c in range(CAP):
                out_box[owner, c * KEY_BLOCK : (c + 1) * KEY_BLOCK, :] = parts[
                    slots_ref[h, owner * CAP + c]
                ]
            return carry

        lax.fori_loop(1, kv_count, to_owner, 0)

    def keep(h):
        def to_self(b, carry):
            total = parts[own_ref[h, b * steps]].astype(F32)
            for step in range(1, steps):
                total += parts[own_ref[h, b * steps + step]].astype(F32)
            at = pl.ds(pl.multiple_of(b * KEY_BLOCK, KEY_BLOCK), KEY_BLOCK)
            kept_ref[at, h * wide : (h + 1) * wide] = total
            return carry

        lax.fori_loop(0, blocks_here, to_self, 0)

    def send_boxes(h, near):
        for dy in range(1) if near else range(1, ny):
            for dz in range(1 if dy == 0 else 0, nz):
                exchange(h, dz, dy).start()

    def weigh(h, i):
        lane = min(256, head_cols)

        def one(c, carry):
            at = pl.ds(pl.multiple_of(c * lane, lane), lane)
            mine = pl.ds(pl.multiple_of(y * tokens, tokens), tokens)
            from_self = pl.ds(pl.multiple_of(h * head_cols + c * lane, lane), lane)
            total = dot_nn(turned[i, :, mine], dq_ref[:, from_self])
            for d in range(1, ny):
                theirs = pl.ds(pl.multiple_of(lax.rem(y + ny - d, ny) * tokens, tokens), tokens)
                total += dot_nn(turned[i, :, theirs], dq_far[h, d - 1, :, at])
            if i < nz - 1:
                partial[i, :, at] = total
            else:
                gw_ref[:, from_self] = total
            return carry

        lax.fori_loop(0, head_cols // lane, one, 0)

    def sum_first(h):
        for d in range(1, ny):
            dq_copy(h, d).wait_recv()
        for i in range(nz):
            weigh(h, i)
            if i < nz - 1:
                @pl.when(jnp.logical_not(has_in(i)))
                def _():
                    z_out[h, i] = partial[i].astype(BF16)
                    sum_copy(h, i).start()

    def sum_relay(h, i):
        @pl.when(has_in(i))
        def _():
            sum_came(h, in_slot(i)).wait_recv()
            z_out[h, i] = (partial[i] + z_in[h, in_slot(i)].astype(F32)).astype(BF16)
            sum_copy(h, i).start()

    def sum_last(h):
        at = slice(h * head_cols, (h + 1) * head_cols)
        for slot, some in ((0, z > 0), (nz, z < nz - 1)):
            @pl.when(some)
            def _():
                sum_came(h, slot).wait_recv()
                gw_ref[:, at] += z_in[h, slot].astype(F32)

    half = max(steps * 3 // 4, 1)
    pool_steps(0, 0, half)
    relay_keys(0, 1)
    pool_steps(0, half, steps)
    for h in range(1, heads):
        pool_steps(h, 0, steps)
    relay_keys(0, 2)
    if heads > 1:
        pass_z(1, 0, 0)
        pass_z(1, 1, 0)
    for h in range(heads):
        pool_out[:, :, h * wide : (h + 1) * wide] = (
            pool_acc[h].astype(BF16).reshape(kv_count, pool_here, wide)
        )
    for s in range(3, nz):
        relay_keys(0, s)
    for row in range(nz):
        for d in range(1, ny):
            hy_copy(d, row).start()
    if heads > 1:
        pass_y(1, 0, 0)
    pool_grads = spread(lambda to: pool_out.at[to], pool_got, pg_send, pg_recv)
    for copy in pool_grads:
        copy.start()
    own_pool = pltpu.make_async_copy(pool_out.at[me], pool_got.at[me], in_sem.at[0])
    own_pool.start()
    hidden_on(0)

    for h in range(heads):
        if h + 1 < heads:
            relay_keys(h + 1, 1)
        keys_complete(h)
        cuts = [steps * (i + 1) // nz for i in range(nz)]
        low = 0
        for i, cut in enumerate(cuts):
            pick_steps(h, low, cut)
            low = cut
            if h > 0 and i < nz - 1:
                sum_relay(h - 1, i)
            if i == nz // 2 and nz > 2:
                relay_keys(h + 1, 2)
        for d in range(1, ny):
            dq_copy(h, d).start()
        if h > 0:
            for dz in range(nz):
                for dy in range(ny):
                    if dz or dy:
                        exchange(h - 1, dz, dy).wait_send()
        pack(h)
        send_boxes(h, True)
        if h + 1 < heads:
            for s in range(3, nz):
                relay_keys(h + 1, s)
            if h + 2 < heads:
                pass_z(h + 2, 0, 0)
                pass_z(h + 2, 1, 0)
                pass_y(h + 2, 0, 0)
        send_boxes(h, False)
        keep(h)
        if h == 0:
            for d in range(1, ny):
                for row in range(nz):
                    hy_copy(d, row).wait_recv()
                hidden_out(d)
            for d in range(1, ny):
                hidden_on(d)
            if cores > 1:
                for e in range(ny):
                    for d in range(nx):
                        hs_copy(e, d).wait_recv()
            for i in range(nz):
                grab = pltpu.make_async_copy(hid_all.at[owner_row(i)], tile, in_sem.at[1])
                grab.start()
                grab.wait()
                turned[i] = tile[...].T
        sum_first(h)
    for i in range(nz - 1):
        sum_relay(heads - 1, i)
    for h in range(heads):
        sum_last(h)

    own_pool.wait()
    for copy in pool_sends:
        copy.wait_send()
    for copy in want_sends + pool_grads:
        copy.wait()
    for h in range(heads):
        for s in range(nz):
            for side in range(2):
                @pl.when(there(side, s))
                def _():
                    @pl.when(onward(side))
                    def _():
                        for p in range(2):
                            z_copy(h, p, side, s, place(side, s)).wait_send()

                    if s > 0 or side == 0:
                        for p in range(2):
                            for d in range(1, ny):
                                y_copy(h, p, side, s, d, place(side, s), y).wait_send()

        for d in range(1, ny):
            dq_copy(h, d).wait_send()
        for dz in range(nz):
            for dy in range(ny):
                if dz or dy:
                    if h == heads - 1:
                        exchange(h, dz, dy).wait_send()
                    exchange(h, dz, dy).wait_recv()
        for i in range(nz - 1):
            sum_copy(h, i).wait_send()
    for d in range(1, ny):
        for row in range(nz):
            hy_copy(d, row).wait_send()
    for e in range(ny):
        for d in range(1, nx):
            hx_copy(e, d).wait_send()
        if cores > 1:
            for d in range(nx):
                hs_copy(e, d).wait_send()


def settle_kernel(
    kv_count, place_ref, asked_ref, got_ref, pool_ref, kept_ref, gk_ref, gv_ref, acc
):
    head = pl.program_id(0)
    tokens = kept_ref.shape[0]
    pool_here = tokens // POOL_BLOCK
    box = CAP * KEY_BLOCK
    pooled = sum(pool_ref[i].astype(F32) for i in range(kv_count)) / POOL_BLOCK
    for j in range(pool_here):
        rows = slice(j * POOL_BLOCK, (j + 1) * POOL_BLOCK)
        acc[rows, :] = kept_ref[rows, :] + pooled[j : j + 1, :]

    def source(i, carry):
        other = lax.rem(place_ref[0] + 1 + i, kv_count)
        for c in range(CAP):
            block = asked_ref[other, head * CAP + c]
            rows = pl.ds(pl.multiple_of(block * KEY_BLOCK, KEY_BLOCK), KEY_BLOCK)
            came = pl.ds(pl.multiple_of(other * box + c * KEY_BLOCK, KEY_BLOCK), KEY_BLOCK)
            acc[rows, :] += got_ref[0, came, :].astype(F32)
        return carry

    lax.fori_loop(0, kv_count - 1, source, 0)
    gk_ref[...] = acc[:, :HEAD_DIM].astype(BF16)
    gv_ref[...] = acc[:, HEAD_DIM:].astype(BF16)


def body(hidden_rows, queries, key_rows, value_rows, branch_gates, log_sums, chosen, out_grad):
    kv_count = lax.axis_size("kv")
    tp_count = lax.axis_size("tp")
    kv_index = lax.axis_index("kv")
    tokens = queries.shape[0]
    kv_local = key_rows.shape[1] // HEAD_DIM
    group = HEADS // KV_HEADS
    scale = HEAD_DIM ** (-0.5)
    seq_len = tokens * kv_count
    steps = tokens // QUERY_BLOCK
    blocks_here = tokens // KEY_BLOCK
    pool_here = tokens // POOL_BLOCK
    request_count = steps * CHOSEN
    slot_count = kv_count * CAP
    nz, ny = grid_of(kv_count)

    lists = chosen.reshape(kv_local, request_count)
    owners = lists // blocks_here
    local_block = lists % blocks_here
    remote = owners != kv_index
    order = jnp.arange(request_count, dtype=jnp.int32)
    rank_in = jnp.sum(
        (
            (owners[:, :, None] == owners[:, None, :]) & (order[None, None, :] < order[None, :, None])
        ).astype(jnp.int32),
        axis=-1,
    )
    slot_index = jnp.where(remote, owners * CAP + rank_in, slot_count)
    hit = slot_index[:, None, :] == jnp.arange(slot_count, dtype=jnp.int32)[None, :, None]
    slot_from = request_count + jnp.sum(jnp.where(hit, order - request_count, 0), axis=-1)
    wanted = jnp.sum(jnp.where(hit, local_block[:, None, :], 0), axis=-1)
    wanted = (
        wanted.reshape(kv_local, kv_count, CAP).transpose(1, 0, 2).reshape(kv_count, 1, -1)
    )
    wanted = jnp.pad(wanted, ((0, 0), (0, 0), (0, 128 - kv_local * CAP)))
    own_block = jnp.where(remote, -1, local_block).reshape(kv_local, 1, steps, CHOSEN)
    same = own_block == jnp.arange(blocks_here, dtype=jnp.int32)[None, :, None, None]
    own_from = (
        request_count
        + jnp.sum(jnp.where(same, order.reshape(steps, CHOSEN) - request_count, 0), axis=-1)
    ).reshape(kv_local, blocks_here * steps)
    place = kv_index.astype(jnp.int32).reshape(1)

    wide = 2 * HEAD_DIM
    box = CAP * KEY_BLOCK
    model = hidden_rows.shape[1]
    out_rows = model // kv_count
    head_cols = group * HEAD_DIM
    out_cols = kv_local * head_cols
    far = max(ny - 1, 1)
    cores = 2 if tp_count % 2 == 0 else 1
    nx = tp_count // cores
    side = max(nx - 1, 1)
    dma = pltpu.SemaphoreType.DMA
    anywhere = pl.BlockSpec(memory_space=pl.ANY)
    inside = pl.BlockSpec(memory_space=pltpu.VMEM)
    scalars = pl.BlockSpec(memory_space=pltpu.SMEM)
    vmem = pltpu.VMEM
    out = jax.ShapeDtypeStruct
    grad_queries, grad_weight, kept, got, pool_got, asked, _ = pl.pallas_call(
        functools.partial(step_kernel, kv_count, tp_count, group, scale),
        in_specs=[scalars] * 3 + [inside] * 6 + [anywhere] * 2,
        out_specs=[inside, inside, inside, anywhere, anywhere, inside, anywhere],
        out_shape=[
            out((tokens, out_cols), BF16),
            out((out_rows, out_cols), F32),
            out((tokens, kv_local * wide), F32),
            out((kv_local, kv_count * box, wide), BF16),
            out((kv_count, pool_here, kv_local * wide), BF16),
            out((kv_count, 1, 128), jnp.int32),
            out((nz, ny * tokens, out_rows), BF16),
        ],
        scratch_shapes=[
            vmem((tokens, out_cols), BF16),
            vmem((tokens, out_cols), BF16),
            [vmem((seq_len // KEY_BLOCK, KEY_BLOCK, HEAD_DIM), BF16) for _ in range(kv_local)],
            [vmem((seq_len // KEY_BLOCK, KEY_BLOCK, HEAD_DIM), BF16) for _ in range(kv_local)],
            vmem((kv_count, pool_here, kv_local * wide), BF16),
            vmem((kv_local, kv_count * pool_here, wide), F32),
            vmem((kv_count, pool_here, kv_local * wide), BF16),
            vmem((kv_local * steps, HEAD_DIM, group * QUERY_BLOCK), F32),
            vmem((kv_local, far, tokens, head_cols), BF16),
            vmem((request_count + 1, KEY_BLOCK, wide), BF16),
            vmem((kv_count, box, wide), BF16),
            vmem((nz, out_rows, ny * tokens), BF16),
            vmem((ny * tokens, out_rows), BF16),
            vmem((max(nz - 1, 1), out_rows, head_cols), F32),
            vmem((kv_local, max(nz - 1, 1), out_rows, head_cols), BF16),
            vmem((kv_local, nz + 1, out_rows, head_cols), BF16),
            dma((3 + 2 * kv_local + nz,)),
            dma((kv_local, 2, 2, nz)), dma((kv_local, 2, 2, nz + 1)),
            dma((kv_local, 2, 2, nz, far)), dma((kv_local, 2, 2, nz, far)),
            dma((kv_count,)), dma((kv_count,)), dma((kv_count,)), dma((kv_count,)),
            dma((kv_count,)), dma((kv_count,)),
            dma((far, nz)), dma((far, nz)), dma((ny, side)), dma((ny, side)),
            dma((ny, nx)), dma((ny, nx)), dma((kv_local, far)), dma((kv_local, far)),
            dma((kv_local, kv_count)), dma((kv_local, kv_count)),
            dma((kv_local, nz)), dma((kv_local, nz + 1)),
        ],
        compiler_params=pltpu.CompilerParams(
            collective_id=0, has_side_effects=True, vmem_limit_bytes=VMEM_LIMIT
        ),
        name="step",
    )(
        lists, slot_from, own_from,
        wanted,
        key_rows.reshape(blocks_here, KEY_BLOCK, kv_local * HEAD_DIM),
        value_rows.reshape(blocks_here, KEY_BLOCK, kv_local * HEAD_DIM),
        hidden_rows, branch_gates, log_sums, queries, out_grad,
    )

    grad_keys, grad_values = pl.pallas_call(
        functools.partial(settle_kernel, kv_count),
        grid_spec=pltpu.PrefetchScalarGridSpec(
            num_scalar_prefetch=2,
            grid=(kv_local,),
            in_specs=[
                pl.BlockSpec((1, kv_count * box, wide), lambda h, *_: (h, 0, 0)),
                pl.BlockSpec((kv_count, pool_here, wide), lambda h, *_: (0, 0, h)),
                pl.BlockSpec((tokens, wide), lambda h, *_: (0, h)),
            ],
            out_specs=[
                pl.BlockSpec((tokens, HEAD_DIM), lambda h, *_: (0, h)),
                pl.BlockSpec((tokens, HEAD_DIM), lambda h, *_: (0, h)),
            ],
            scratch_shapes=[pltpu.VMEM((tokens, wide), F32)],
        ),
        out_shape=[
            jax.ShapeDtypeStruct((tokens, kv_local * HEAD_DIM), BF16),
            jax.ShapeDtypeStruct((tokens, kv_local * HEAD_DIM), BF16),
        ],
        cost_estimate=pl.CostEstimate(
            flops=4 * 2**20, bytes_accessed=8 * 2**20, transcendentals=0
        ),
        name="settle",
    )(place, asked.reshape(kv_count, 128), got, pool_got, kept)
    return (grad_queries, grad_keys, grad_values, grad_weight)


def solution(mesh):
    placed = (
        P(("kv", "tp"), None),
        P("kv", "tp"),
        P("kv", "tp"),
        P("kv", "tp"),
        P(None, "tp", "kv"),
        P(None, "tp", "kv"),
        P("tp", "kv", None),
        P("kv", "tp"),
    )
    return jax.shard_map(
        body,
        mesh=mesh,
        in_specs=placed,
        out_specs=(P("kv", "tp"), P("kv", "tp"), P("kv", "tp"), P("kv", "tp")),
        check_vma=False,
    )
```

time: 452 us -> 289 us (0.64)
  waiting for transfers between devices: 349 us -> 0 us
  Pallas kernels: 48.8 us -> 281 us
  matrix products: 14.9 us -> 0 us
  between operations: 13.8 us -> 0.71 us
  blocking collectives: 11.9 us -> 0 us
  starting transfers between devices: 4.7 us -> 0 us
  other arithmetic: 6.46 us -> 1.8 us
    pallas_call x2, Pallas kernels: 48.8 us -> 281 us  [the longest x1 275 us: body(): pl.pallas_call(functools.partial(step_kernel, kv_count, tp_count, group,...]
    all_to_all x1 -> x0, waiting for transfers between devices: 156 us -> none  [body(): got = lax.all_to_all(send, 'kv', split_axis=0, concat_axis=0, tiled=True)]
    all_gather x2 -> x0, waiting for transfers between devices: 140 us -> none  [the longest x1 128 us: body(): every_pair = lax.all_gather(pair_rows, 'kv', axis=0, tiled=True)]
    reduce_scatter x1 -> x0, waiting for transfers between devices: 53 us -> none  [body(): lax.psum_scatter(terms, 'kv', scatter_dimension=0, tiled=True).astype(F32)]
    dot_general x1 -> x0, matrix products: 14.9 us -> none  [body(): lax.dot_general(whole_rows, grad_queries, (((0,), (0,)), ((), ())), prefe...]
    all_to_all x1 -> x0, blocking collectives: 11.9 us -> none  [body(): lax.all_to_all(wanted, 'kv', split_axis=1, concat_axis=1, tiled=True)]
    all_to_all x1 -> x0, starting transfers between devices: 4.58 us -> none  [body(): got = lax.all_to_all(send, 'kv', split_axis=0, concat_axis=0, tiled=True)]
  transfers between devices with their start and end apart: 4 -> 0, of which waited for: 4 -> 0; matrix products, arithmetic and copies ran while one was open for 1% -> 0% of each run, Pallas kernels for 11% -> 0%
where the time goes in v2:
time: 289 us
  Pallas kernels  281 us (97%)
  local copies, waits for them, and re-layouts  5.98 us (2%)
    pallas_call x1, Pallas kernels, body(): pl.pallas_call(functools.partial(step_kernel, kv_count, tp_count, group,...  275 us

profile of v2, /device:TPU:0, one launch (start us, length us, event | category | flops | bytes accessed | tf_op | source)
XLA Modules:
  0.0 289.0 jit_solution(16924597941708329034)
XLA Ops:
  0.6 0.8 reshape.178.lists_ref
  1.4 0.0 copy-start.2
  1.5 0.7 fusion.1
  2.2 0.1 select_reduce_fusion.1
  2.3 0.2 convert_reduce_fusion
  2.5 0.1 select_reduce_fusion
  2.7 0.6 broadcast_add_fusion.1.slots_ref
  3.3 0.1 reshape.182
  3.3 0.1 reshape.183
  3.4 0.6 pad.4.wanted_ref
  4.0 0.1 copy.13
  4.1 0.7 add.59.own_ref
  4.8 0.0 copy-done.2
  4.8 275.0 %step.1 = (bf16[1024,1024]{1,0:T(8,128)(2,1)}, f32[512,1024]{1,0:T(8,128)}, f32[1024,512]{1,0:T(8,128)}, bf16[2,4096,256]{2,1,0:T(8,128)(2,1)}, bf16[8,32,512]{2...) custom-call(s32[2,128]{1,0:T(2,128)} %copy-done.2, s32[2,128]{1,0:T(2,128)} %broadcast_add_fusion.1.slots_ref, ...), custom_call_target="tpu_custom_call" | custom-call | tf_op jit(solution)/shard_map/step/pallas_call | solution.py:663
  279.9 0.0 copy-start.1
  279.9 5.5 %settle.1 = (bf16[1024,256]{1,0:T(8,128)(2,1)}, bf16[1024,256]{1,0:T(8,128)(2,1)}) custom-call(s32[1]{0:T(128)} %bitcast.3.place_ref, s32[8,128]{1,0:T(8,128)} %bitcast.8, bf16[2,4096,256]{2,1,0:T(8,128)(2,1)} %get-tuple-element.14.got_ref, bf16[8,32,512]{2,1,0:T(8,128)(2,1)} %get-tuple-element.15.pool_ref, f32[1024,512]{1,0:T(8,128)} %get-tuple-element.16.kept_ref), custom_call_target="tpu_custom_call" | custom-call | flops 4194304 | bytes 8388608 | tf_op jit(solution)/shard_map/settle/pallas_call | solution.py:715
  285.4 0.0 copy-done.1
  285.4 0.0 copy-start
  285.4 1.3 copy.17
  286.7 1.0 copy-done
  287.7 1.3 copy.18
  (7 shorter events, 0.1 us)
Async XLA Ops:
  1.4 3.4 %copy-start.2 = (s32[2,128]{1,0:T(2,128)}, s32[2,128]{1,0:T(2,128)S(1)}, u32[]{:S(2)}) copy-start(s32[2,128]{1,0:T(2,128)S(1)} %reshape.178.lists_ref) | copy-start | bytes 3076
  279.9 5.5 %copy-start.1 = (bf16[1024,1024]{1,0:T(8,128)(2,1)S(1)}, bf16[1024,1024]{1,0:T(8,128)(2,1)}, u32[]{:S(2)}) copy-start(bf16[1024,1024]{1,0:T(8,128)(2,1)} %get-tuple-element.28) | copy-start | bytes 6291460
  285.4 2.3 copy-start

commit v3 on v2

--- a/solution.py
+++ b/solution.py
@@ -19,7 +19,7 @@
 F32 = jnp.float32
 BF16 = jnp.bfloat16
 MESH = pl.DeviceIdType.MESH
-VMEM_LIMIT = 62 * 2**20
+VMEM_LIMIT = 67043328
 
 
 def dot_nt(a, b):
@@ -59,12 +59,14 @@
 
 def step_kernel(
     kv_count, tp_count, group, scale,
-    lists_ref, slots_ref, own_ref,
-    wanted_ref, k_ref, v_ref, hidden_ref, gate_ref, log_ref, q_hbm, g_hbm,
+    lists_ref, spots_ref, slots_ref, own_ref,
+    wanted_ref, k_ref, v_ref, gate_ref, log_ref, hidden_ref, q_hbm, g_hbm,
     dq_ref, gw_ref, kept_ref, got_ref, pool_got, asked_ref, hid_all,
-    q_buf, g_buf, k_heads, v_heads, pooled, pool_acc, pool_out, dq_pool, dq_far,
+    q_buf, g_buf, kv_all, kv_own, kv_in, kv_out, want_in, want,
+    pooled, pool_acc, pool_out, dq_pool, dq_far,
     parts, out_box, turned, tile, partial, z_out, z_in,
-    in_sem, z_send, z_recv, y_send, y_recv, p_send, p_recv, w_send, w_recv, pg_send, pg_recv,
+    in_sem, z_send, z_recv, y_send, y_recv, t_send, t_recv,
+    p_send, p_recv, w_send, w_recv, pg_send, pg_recv,
     hy_send, hy_recv, hx_send, hx_recv, hs_send, hs_recv, dq_send, dq_recv,
     a_send, a_recv, s_send, s_recv,
 ):
@@ -90,11 +92,14 @@
     wide = 2 * HEAD_DIM
     width = group * QUERY_BLOCK
     box = CAP * KEY_BLOCK
+    own_keys = (k_ref, v_ref)
+    for h in range(heads):
+        for p in range(2):
+            kv_own[h, p] = own_keys[p][:, :, h * HEAD_DIM : (h + 1) * HEAD_DIM]
     meet(
         [{"kv": lax.rem(me + d, kv_count)} for d in range(1, kv_count)]
         + [{"tp": lax.rem(tp + d, tp_count)} for d in range(1, tp_count)]
     )
-    banks = ((k_ref, k_heads), (v_ref, v_heads))
 
     def remote(src, dst, send, recv, to):
         return pltpu.make_async_remote_copy(
@@ -102,25 +107,27 @@
             device_id=to, device_id_type=MESH,
         )
 
-    def rows_of(row, col):
-        return pl.ds((row * ny + col) * blocks_here, blocks_here)
-
-    def source(h, p, s, row):
-        if s == 0:
-            return banks[p][0].at[:, :, h * HEAD_DIM : (h + 1) * HEAD_DIM]
-        return banks[p][1][h].at[rows_of(row, y)]
-
-    def z_copy(h, p, side, s, row):
+    def source(h, side, s):
+        return kv_own.at[h] if s == 0 else kv_in[h][side][s - 1]
+
+    def z_copy(h, side, s):
         to = z + 1 if side == 0 else z - 1
         return remote(
-            source(h, p, s, row), banks[p][1][h].at[rows_of(row, y)],
-            z_send.at[h, p, side, s], z_recv.at[h, p, side, s + 1], {"kv": to * ny + y},
-        )
-
-    def y_copy(h, p, side, s, d, row, col):
-        return remote(
-            source(h, p, s, row), banks[p][1][h].at[rows_of(row, col)],
-            y_send.at[h, p, side, s, d - 1], y_recv.at[h, p, side, s, d - 1],
+            source(h, side, s), kv_in[h][side][s],
+            z_send.at[h, side, s], z_recv.at[h, side, s], {"kv": to * ny + y},
+        )
+
+    def y_copy(h, row, d):
+        at = nz * blocks_here + (row * (ny - 1) + d - 1) * CAP
+        return remote(
+            kv_out.at[h, row, d - 1], kv_all[h].at[:, pl.ds(at, CAP)],
+            y_send.at[h, row, d - 1], y_recv.at[h, row, d - 1],
+            {"kv": z * ny + lax.rem(y + d, ny)},
+        )
+
+    def t_copy(d):
+        return remote(
+            wanted_ref, want_in.at[d - 1], t_send.at[d - 1], t_recv.at[d - 1],
             {"kv": z * ny + lax.rem(y + d, ny)},
         )
 
@@ -130,19 +137,22 @@
     def onward(side):
         return z < nz - 1 if side == 0 else z > 0
 
-    def place(side, s):
-        return z - s if side == 0 else z + s
-
     def pass_z(h, side, s):
-        @pl.when(onward(side))
-        def _():
-            for p in range(2):
-                z_copy(h, p, side, s, place(side, s)).start()
+        if s < nz - 1:
+            @pl.when(onward(side))
+            def _():
+                z_copy(h, side, s).start()
 
     def pass_y(h, side, s):
-        for p in range(2):
-            for d in range(1, ny):
-                y_copy(h, p, side, s, d, place(side, s), y).start()
+        row = z - s if side == 0 else z + s
+        held = source(h, side, s)
+        kv_all[h][:, pl.ds(row * blocks_here, blocks_here)] = held[...]
+        for d in range(1, ny):
+            for c in range(CAP):
+                block = want[ny - d - 1, row * ny + y, 0, h * CAP + c]
+                for p in range(2):
+                    kv_out[h, row, d - 1, p, c] = held[p, block]
+            y_copy(h, row, d).start()
 
     def relay_keys(h, s):
         if h >= heads:
@@ -150,19 +160,18 @@
         for side in range(2):
             @pl.when(there(side, s))
             def _():
-                for p in range(2):
-                    z_copy(h, p, side, s - 1, place(side, s)).wait_recv()
+                z_copy(h, side, s - 1).wait_recv()
                 pass_z(h, side, s)
+
+        for side in range(2):
+            @pl.when(there(side, s))
+            def _():
                 pass_y(h, side, s)
 
     def keys_complete(h):
-        for s in range(nz):
-            for side in range(1 if s == 0 else 2):
-                @pl.when(there(side, s))
-                def _():
-                    for p in range(2):
-                        for d in range(1, ny):
-                            y_copy(h, p, side, s, d, place(side, s), y).wait_recv()
+        for row in range(nz):
+            for d in range(1, ny):
+                y_copy(h, row, d).wait_recv()
 
     def others(make):
         return [make(d) for d in range(1, kv_count)]
@@ -179,19 +188,22 @@
         pltpu.make_async_copy(g_hbm, g_buf, in_sem.at[1]),
         pltpu.make_async_copy(wanted_ref.at[me], asked_ref.at[me], in_sem.at[2]),
     ]
-    for h in range(heads):
-        for p in range(2):
-            fetches.append(
-                pltpu.make_async_copy(
-                    source(h, p, 0, z), banks[p][1][h].at[rows_of(z, y)],
-                    in_sem.at[3 + 2 * h + p],
-                )
-            )
+    def hid_piece(row):
+        return tile.at[row * hidden_rows : (row + 1) * hidden_rows]
+
     hid_local = [
         pltpu.make_async_copy(
             hidden_ref.at[:, pl.ds(pl.multiple_of((row * ny + y) * rows, rows), rows)],
+            hid_piece(row),
+            in_sem.at[3 + row],
+        )
+        for row in range(nz)
+    ]
+    hid_home = [
+        pltpu.make_async_copy(
+            hid_piece(row),
             hid_all.at[row, pl.ds(pl.multiple_of((y * tp_count + tp) * hidden_rows, hidden_rows), hidden_rows)],
-            in_sem.at[3 + 2 * heads + row],
+            in_sem.at[3 + row],
         )
         for row in range(nz)
     ]
@@ -283,29 +295,47 @@
     def has_in(i):
         return jnp.where(goes_right(i), jnp.where(z > 0, 1, 0), jnp.where(z < nz - 1, 1, 0)) > 0
 
+    pass_z(0, 0, 0)
+    pass_z(0, 1, 0)
+    for d in range(1, ny):
+        t_copy(d).start()
     pick = (
         lax.broadcasted_iota(jnp.int32, (pool_here, tokens), 1) // POOL_BLOCK
         == lax.broadcasted_iota(jnp.int32, (pool_here, tokens), 0)
     ).astype(BF16)
     for p in range(2):
-        mean = (dot_nn(pick, banks[p][0][...].reshape(tokens, heads * HEAD_DIM)) / POOL_BLOCK).astype(BF16)
+        all_rows = own_keys[p][...].reshape(tokens, heads * HEAD_DIM)
+        mean = (dot_nn(pick, all_rows) / POOL_BLOCK).astype(BF16)
         pooled[me, :, p * heads * HEAD_DIM : (p + 1) * heads * HEAD_DIM] = mean
     pool_sends = spread(lambda to: pooled.at[me], pooled, p_send, p_recv)
     for copy in pool_sends:
         copy.start()
     want_sends = spread(lambda to: wanted_ref.at[to], asked_ref, w_send, w_recv)
-    pass_z(0, 0, 0)
-    pass_z(0, 1, 0)
-    pass_y(0, 0, 0)
     for copy in fetches + hid_local + want_sends:
         copy.start()
     parts[requests] = jnp.zeros((KEY_BLOCK, wide), BF16)
     pool_acc[...] = jnp.zeros_like(pool_acc)
-    for copy in hid_local:
+    for there_copy, home_copy in zip(hid_local, hid_home):
+        there_copy.wait()
+        home_copy.start()
+    for copy in hid_home:
         copy.wait()
     hidden_out(0)
+    for d in range(1, ny):
+        t_copy(d).wait_recv()
     for copy in fetches:
         copy.wait()
+    to_scalar = pltpu.make_async_copy(want_in, want, in_sem.at[0])
+    to_scalar.start()
+    to_scalar.wait()
+    pass_y(0, 0, 0)
+
+    def hy_start(row):
+        if row < nz:
+            for d in range(1, ny):
+                hy_copy(d, row).start()
+
+    hy_start(0)
     for copy in pool_sends:
         copy.wait_recv()
 
@@ -361,8 +391,9 @@
         def one(b, carry):
             at, stack, cots, log_row, query_pos = load_step(h, b, 1)
             ids = [lists_ref[h, b * CHOSEN + c] for c in range(CHOSEN)]
-            keys = jnp.concatenate([k_heads[h][i] for i in ids], axis=0)
-            values = jnp.concatenate([v_heads[h][i] for i in ids], axis=0)
+            spots = [spots_ref[h, b * CHOSEN + c] for c in range(CHOSEN)]
+            keys = jnp.concatenate([kv_all[h][0, i] for i in spots], axis=0)
+            values = jnp.concatenate([kv_all[h][1, i] for i in spots], axis=0)
             offset = lax.broadcasted_iota(jnp.int32, (KEY_BLOCK, width), 0)
             key_pos = jnp.concatenate([offset + i * KEY_BLOCK for i in ids], axis=0)
             dq, dk, dv = branch_back(
@@ -456,24 +487,21 @@
     half = max(steps * 3 // 4, 1)
     pool_steps(0, 0, half)
     relay_keys(0, 1)
+    hy_start(1)
     pool_steps(0, half, steps)
     for h in range(1, heads):
         pool_steps(h, 0, steps)
-    relay_keys(0, 2)
-    if heads > 1:
-        pass_z(1, 0, 0)
-        pass_z(1, 1, 0)
+    for s in range(2, nz):
+        relay_keys(0, s)
+        hy_start(s)
+        if s == 2 and heads > 1:
+            pass_z(1, 0, 0)
+            pass_z(1, 1, 0)
+            pass_y(1, 0, 0)
     for h in range(heads):
         pool_out[:, :, h * wide : (h + 1) * wide] = (
             pool_acc[h].astype(BF16).reshape(kv_count, pool_here, wide)
         )
-    for s in range(3, nz):
-        relay_keys(0, s)
-    for row in range(nz):
-        for d in range(1, ny):
-            hy_copy(d, row).start()
-    if heads > 1:
-        pass_y(1, 0, 0)
     pool_grads = spread(lambda to: pool_out.at[to], pool_got, pg_send, pg_recv)
     for copy in pool_grads:
         copy.start()
@@ -481,18 +509,43 @@
     own_pool.start()
     hidden_on(0)
 
+    def hidden_arrived():
+        for d in range(1, ny):
+            for row in range(nz):
+                hy_copy(d, row).wait_recv()
+            hidden_out(d)
+
+    def hidden_ready():
+        for d in range(1, ny):
+            hidden_on(d)
+        if cores > 1:
+            for e in range(ny):
+                for d in range(nx):
+                    hs_copy(e, d).wait_recv()
+        for i in range(nz):
+            for col in range(ny):
+                at = pl.ds(col * tokens, tokens)
+                grab = pltpu.make_async_copy(hid_all.at[owner_row(i), at], tile, in_sem.at[1])
+                grab.start()
+                grab.wait()
+                turned[i, :, col * tokens : (col + 1) * tokens] = tile[...].T
+
     for h in range(heads):
-        if h + 1 < heads:
-            relay_keys(h + 1, 1)
         keys_complete(h)
-        cuts = [steps * (i + 1) // nz for i in range(nz)]
+        cuts = [max(steps // 4, 1), max(steps // 2, 1), steps * 7 // 8, steps]
         low = 0
-        for i, cut in enumerate(cuts):
-            pick_steps(h, low, cut)
-            low = cut
-            if h > 0 and i < nz - 1:
-                sum_relay(h - 1, i)
-            if i == nz // 2 and nz > 2:
+        for i, high in enumerate(cuts):
+            pick_steps(h, low, high)
+            low = high
+            if h > 0:
+                sums = [j for j in range(nz - 1) if min(j, 2) == i]
+                for j in sums:
+                    sum_relay(h - 1, j)
+            if i == 0:
+                relay_keys(h + 1, 1)
+                if h == 0:
+                    hidden_arrived()
+            if i == 2:
                 relay_keys(h + 1, 2)
         for d in range(1, ny):
             dq_copy(h, d).start()
@@ -503,32 +556,17 @@
                         exchange(h - 1, dz, dy).wait_send()
         pack(h)
         send_boxes(h, True)
-        if h + 1 < heads:
-            for s in range(3, nz):
-                relay_keys(h + 1, s)
-            if h + 2 < heads:
-                pass_z(h + 2, 0, 0)
-                pass_z(h + 2, 1, 0)
-                pass_y(h + 2, 0, 0)
-        send_boxes(h, False)
+        for s in range(3, nz):
+            relay_keys(h + 1, s)
+        if h + 2 < heads:
+            pass_z(h + 2, 0, 0)
+            pass_z(h + 2, 1, 0)
+            pass_y(h + 2, 0, 0)
         keep(h)
         if h == 0:
-            for d in range(1, ny):
-                for row in range(nz):
-                    hy_copy(d, row).wait_recv()
-                hidden_out(d)
-            for d in range(1, ny):
-                hidden_on(d)
-            if cores > 1:
-                for e in range(ny):
-                    for d in range(nx):
-                        hs_copy(e, d).wait_recv()
-            for i in range(nz):
-                grab = pltpu.make_async_copy(hid_all.at[owner_row(i)], tile, in_sem.at[1])
-                grab.start()
-                grab.wait()
-                turned[i] = tile[...].T
+            hidden_ready()
         sum_first(h)
+        send_boxes(h, False)
     for i in range(nz - 1):
         sum_relay(heads - 1, i)
     for h in range(heads):
@@ -539,21 +577,20 @@
         copy.wait_send()
     for copy in want_sends + pool_grads:
         copy.wait()
+    for d in range(1, ny):
+        t_copy(d).wait_send()
     for h in range(heads):
-        for s in range(nz):
+        for s in range(nz - 1):
             for side in range(2):
                 @pl.when(there(side, s))
                 def _():
                     @pl.when(onward(side))
                     def _():
-                        for p in range(2):
-                            z_copy(h, p, side, s, place(side, s)).wait_send()
-
-                    if s > 0 or side == 0:
-                        for p in range(2):
-                            for d in range(1, ny):
-                                y_copy(h, p, side, s, d, place(side, s), y).wait_send()
-
+                        z_copy(h, side, s).wait_send()
+
+        for row in range(nz):
+            for d in range(1, ny):
+                y_copy(h, row, d).wait_send()
         for d in range(1, ny):
             dq_copy(h, d).wait_send()
         for dz in range(nz):
@@ -643,6 +680,14 @@
         + jnp.sum(jnp.where(same, order.reshape(steps, CHOSEN) - request_count, 0), axis=-1)
     ).reshape(kv_local, blocks_here * steps)
     place = kv_index.astype(jnp.int32).reshape(1)
+    row, col = owners // ny, owners % ny
+    here = kv_index % ny
+    away = (here - col + ny) % ny
+    spots = jnp.where(
+        away == 0,
+        row * blocks_here + local_block,
+        nz * blocks_here + (row * (ny - 1) + away - 1) * CAP + rank_in,
+    )
 
     wide = 2 * HEAD_DIM
     box = CAP * KEY_BLOCK
@@ -662,7 +707,7 @@
     out = jax.ShapeDtypeStruct
     grad_queries, grad_weight, kept, got, pool_got, asked, _ = pl.pallas_call(
         functools.partial(step_kernel, kv_count, tp_count, group, scale),
-        in_specs=[scalars] * 3 + [inside] * 6 + [anywhere] * 2,
+        in_specs=[scalars] * 4 + [inside] * 5 + [anywhere] * 3,
         out_specs=[inside, inside, inside, anywhere, anywhere, inside, anywhere],
         out_shape=[
             out((tokens, out_cols), BF16),
@@ -676,8 +721,21 @@
         scratch_shapes=[
             vmem((tokens, out_cols), BF16),
             vmem((tokens, out_cols), BF16),
-            [vmem((seq_len // KEY_BLOCK, KEY_BLOCK, HEAD_DIM), BF16) for _ in range(kv_local)],
-            [vmem((seq_len // KEY_BLOCK, KEY_BLOCK, HEAD_DIM), BF16) for _ in range(kv_local)],
+            [
+                vmem((2, nz * (blocks_here + (ny - 1) * CAP), KEY_BLOCK, HEAD_DIM), BF16)
+                for _ in range(kv_local)
+            ],
+            vmem((kv_local, 2, blocks_here, KEY_BLOCK, HEAD_DIM), BF16),
+            [
+                [
+                    [vmem((2, blocks_here, KEY_BLOCK, HEAD_DIM), BF16) for _ in range(nz - 1)]
+                    for _ in range(2)
+                ]
+                for _ in range(kv_local)
+            ],
+            vmem((kv_local, nz, far, 2, CAP, KEY_BLOCK, HEAD_DIM), BF16),
+            vmem((far, kv_count, 1, 128), jnp.int32),
+            pltpu.SMEM((far, kv_count, 1, 128), jnp.int32),
             vmem((kv_count, pool_here, kv_local * wide), BF16),
             vmem((kv_local, kv_count * pool_here, wide), F32),
             vmem((kv_count, pool_here, kv_local * wide), BF16),
@@ -686,13 +744,13 @@
             vmem((request_count + 1, KEY_BLOCK, wide), BF16),
             vmem((kv_count, box, wide), BF16),
             vmem((nz, out_rows, ny * tokens), BF16),
-            vmem((ny * tokens, out_rows), BF16),
+            vmem((tokens, out_rows), BF16),
             vmem((max(nz - 1, 1), out_rows, head_cols), F32),
             vmem((kv_local, max(nz - 1, 1), out_rows, head_cols), BF16),
             vmem((kv_local, nz + 1, out_rows, head_cols), BF16),
-            dma((3 + 2 * kv_local + nz,)),
-            dma((kv_local, 2, 2, nz)), dma((kv_local, 2, 2, nz + 1)),
-            dma((kv_local, 2, 2, nz, far)), dma((kv_local, 2, 2, nz, far)),
+            dma((3 + nz,)),
+            dma((kv_local, 2, nz)), dma((kv_local, 2, nz)),
+            dma((kv_local, nz, far)), dma((kv_local, nz, far)), dma((far,)), dma((far,)),
             dma((kv_count,)), dma((kv_count,)), dma((kv_count,)), dma((kv_count,)),
             dma((kv_count,)), dma((kv_count,)),
             dma((far, nz)), dma((far, nz)), dma((ny, side)), dma((ny, side)),
@@ -705,11 +763,11 @@
         ),
         name="step",
     )(
-        lists, slot_from, own_from,
+        lists, spots, slot_from, own_from,
         wanted,
         key_rows.reshape(blocks_here, KEY_BLOCK, kv_local * HEAD_DIM),
         value_rows.reshape(blocks_here, KEY_BLOCK, kv_local * HEAD_DIM),
-        hidden_rows, branch_gates, log_sums, queries, out_grad,
+        branch_gates, log_sums, hidden_rows, queries, out_grad,
     )
 
     grad_keys, grad_values = pl.pallas_call(

time: 289 us -> 259 us (0.90); the launches traced: 289 us -> 256 us
  Pallas kernels: 281 us -> 247 us
    pallas_call x1, Pallas kernels: 275 us -> 241 us  [body(): pl.pallas_call(functools.partial(step_kernel, kv_count, tp_count, group,...]
where the time goes in v3:
time: 259 us; the launch traced here: 256 us
  Pallas kernels  247 us (95%)
  local copies, waits for them, and re-layouts  5.98 us (2%)
    pallas_call x1, Pallas kernels, body(): pl.pallas_call(functools.partial(step_kernel, kv_count, tp_count, group,...  241 us
    pallas_call x1, Pallas kernels, body(): pl.pallas_call(functools.partial(settle_kernel, kv_count), grid_spec=pltp...  5.48 us

profile of v3, /device:TPU:0, one launch (start us, length us, event | category | flops | bytes accessed | tf_op | source)
XLA Modules:
  0.0 255.9 jit_solution(11382140964018136960)
XLA Ops:
  0.7 0.8 reshape.178.lists_ref
  1.4 0.0 copy-start.2
  1.5 0.7 fusion.1
  2.2 0.1 select_reduce_fusion.1
  2.3 0.2 convert_reduce_fusion
  2.5 0.6 compare_select_fusion.3
  3.1 0.1 select_reduce_fusion
  3.3 0.0 copy-done.2
  3.3 0.5 broadcast_add_fusion.1.slots_ref
  3.8 0.1 reshape.182
  3.9 0.1 reshape.183
  4.0 0.6 pad.4.wanted_ref
  4.6 0.1 copy.13
  4.7 0.7 add.97.own_ref
  5.3 241.4 %step.1 = (bf16[1024,1024]{1,0:T(8,128)(2,1)}, f32[512,1024]{1,0:T(8,128)}, f32[1024,512]{1,0:T(8,128)}, bf16[2,4096,256]{2,1,0:T(8,128)(2,1)}, bf16[8,32,512]{2...) custom-call(s32[2,128]{1,0:T(2,128)} %copy-done.2, s32[2,128]{1,0:T(2,128)} %get-tuple-element.22.spots_ref, ...), custom_call_target="tpu_custom_call" | custom-call | tf_op jit(solution)/shard_map/step/pallas_call | solution.py:708
  246.7 0.0 copy-start.1
  246.7 5.5 %settle.1 = (bf16[1024,256]{1,0:T(8,128)(2,1)}, bf16[1024,256]{1,0:T(8,128)(2,1)}) custom-call(s32[1]{0:T(128)} %bitcast.3.place_ref, s32[8,128]{1,0:T(8,128)} %bitcast.8, bf16[2,4096,256]{2,1,0:T(8,128)(2,1)} %get-tuple-element.14.got_ref, bf16[8,32,512]{2,1,0:T(8,128)(2,1)} %get-tuple-element.15.pool_ref, f32[1024,512]{1,0:T(8,128)} %get-tuple-element.16.kept_ref), custom_call_target="tpu_custom_call" | custom-call | flops 4194304 | bytes 8388608 | tf_op jit(solution)/shard_map/settle/pallas_call | solution.py:773
  252.2 0.0 copy-done.1
  252.2 0.0 copy-start
  252.2 1.3 copy.17
  253.6 1.0 copy-done
  254.6 1.3 copy.18
  (6 shorter events, 0.0 us)
Async XLA Ops:
  1.4 1.8 copy-start.2
  246.7 5.5 %copy-start.1 = (bf16[1024,1024]{1,0:T(8,128)(2,1)S(1)}, bf16[1024,1024]{1,0:T(8,128)(2,1)}, u32[]{:S(2)}) copy-start(bf16[1024,1024]{1,0:T(8,128)(2,1)} %get-tuple-element.29) | copy-start | bytes 6291460
  252.2 2.3 copy-start

commit v4 on v3

--- a/solution.py
+++ b/solution.py
@@ -64,7 +64,7 @@
     dq_ref, gw_ref, kept_ref, got_ref, pool_got, asked_ref, hid_all,
     q_buf, g_buf, kv_all, kv_own, kv_in, kv_out, want_in, want,
     pooled, pool_acc, pool_out, dq_pool, dq_far,
-    parts, out_box, turned, tile, partial, z_out, z_in,
+    parts, out_box, turned, tile, z_out, z_in,
     in_sem, z_send, z_recv, y_send, y_recv, t_send, t_recv,
     p_send, p_recv, w_send, w_recv, pg_send, pg_recv,
     hy_send, hy_recv, hx_send, hx_recv, hs_send, hs_recv, dq_send, dq_recv,
@@ -252,7 +252,7 @@
         to = lax.rem(z + dz, nz) * ny + lax.rem(y + dy, ny)
         n = dz * ny + dy
         return remote(
-            out_box.at[to],
+            out_box.at[h, to],
             got_ref.at[h, pl.ds(pl.multiple_of(me * box, box), box)],
             a_send.at[h, n], a_recv.at[h, n], {"kv": to},
         )
@@ -416,7 +416,7 @@
         def to_owner(d, carry):
             owner = lax.rem(me + d, kv_count)
             for c in range(CAP):
-                out_box[owner, c * KEY_BLOCK : (c + 1) * KEY_BLOCK, :] = parts[
+                out_box[h, owner, c * KEY_BLOCK : (c + 1) * KEY_BLOCK, :] = parts[
                     slots_ref[h, owner * CAP + c]
                 ]
             return carry
@@ -444,14 +444,12 @@
 
         def one(c, carry):
             at = pl.ds(pl.multiple_of(c * lane, lane), lane)
-            mine = pl.ds(pl.multiple_of(y * tokens, tokens), tokens)
             from_self = pl.ds(pl.multiple_of(h * head_cols + c * lane, lane), lane)
-            total = dot_nn(turned[i, :, mine], dq_ref[:, from_self])
+            total = dot_nn(turned[i, 0], dq_ref[:, from_self])
             for d in range(1, ny):
-                theirs = pl.ds(pl.multiple_of(lax.rem(y + ny - d, ny) * tokens, tokens), tokens)
-                total += dot_nn(turned[i, :, theirs], dq_far[h, d - 1, :, at])
+                total += dot_nn(turned[i, d], dq_far[h, d - 1, :, at])
             if i < nz - 1:
-                partial[i, :, at] = total
+                z_out[h, i, :, at] = total.astype(BF16)
             else:
                 gw_ref[:, from_self] = total
             return carry
@@ -466,14 +464,15 @@
             if i < nz - 1:
                 @pl.when(jnp.logical_not(has_in(i)))
                 def _():
-                    z_out[h, i] = partial[i].astype(BF16)
                     sum_copy(h, i).start()
 
     def sum_relay(h, i):
         @pl.when(has_in(i))
         def _():
             sum_came(h, in_slot(i)).wait_recv()
-            z_out[h, i] = (partial[i] + z_in[h, in_slot(i)].astype(F32)).astype(BF16)
+            z_out[h, i] = (
+                z_out[h, i].astype(F32) + z_in[h, in_slot(i)].astype(F32)
+            ).astype(BF16)
             sum_copy(h, i).start()
 
     def sum_last(h):
@@ -515,21 +514,21 @@
                 hy_copy(d, row).wait_recv()
             hidden_out(d)
 
-    def hidden_ready():
-        for d in range(1, ny):
-            hidden_on(d)
+    def hidden_ready(e):
+        if e > 0:
+            hidden_on(e)
         if cores > 1:
-            for e in range(ny):
-                for d in range(nx):
-                    hs_copy(e, d).wait_recv()
+            for d in range(nx):
+                hs_copy(e, d).wait_recv()
+        col = lax.rem(y + ny - e, ny)
+        at = pl.ds(pl.multiple_of(col * tokens, tokens), tokens)
         for i in range(nz):
-            for col in range(ny):
-                at = pl.ds(col * tokens, tokens)
-                grab = pltpu.make_async_copy(hid_all.at[owner_row(i), at], tile, in_sem.at[1])
-                grab.start()
-                grab.wait()
-                turned[i, :, col * tokens : (col + 1) * tokens] = tile[...].T
-
+            grab = pltpu.make_async_copy(hid_all.at[owner_row(i), at], tile, in_sem.at[1])
+            grab.start()
+            grab.wait()
+            turned[i, e] = tile[...].T
+
+    hidden_ready(0)
     for h in range(heads):
         keys_complete(h)
         cuts = [max(steps // 4, 1), max(steps // 2, 1), steps * 7 // 8, steps]
@@ -538,9 +537,9 @@
             pick_steps(h, low, high)
             low = high
             if h > 0:
-                sums = [j for j in range(nz - 1) if min(j, 2) == i]
-                for j in sums:
-                    sum_relay(h - 1, j)
+                for j in range(nz - 1):
+                    if min(j, 2) == i:
+                        sum_relay(h - 1, j)
             if i == 0:
                 relay_keys(h + 1, 1)
                 if h == 0:
@@ -549,11 +548,6 @@
                 relay_keys(h + 1, 2)
         for d in range(1, ny):
             dq_copy(h, d).start()
-        if h > 0:
-            for dz in range(nz):
-                for dy in range(ny):
-                    if dz or dy:
-                        exchange(h - 1, dz, dy).wait_send()
         pack(h)
         send_boxes(h, True)
         for s in range(3, nz):
@@ -562,11 +556,12 @@
             pass_z(h + 2, 0, 0)
             pass_z(h + 2, 1, 0)
             pass_y(h + 2, 0, 0)
+        send_boxes(h, False)
         keep(h)
         if h == 0:
-            hidden_ready()
+            for e in range(1, ny):
+                hidden_ready(e)
         sum_first(h)
-        send_boxes(h, False)
     for i in range(nz - 1):
         sum_relay(heads - 1, i)
     for h in range(heads):
@@ -596,9 +591,7 @@
         for dz in range(nz):
             for dy in range(ny):
                 if dz or dy:
-                    if h == heads - 1:
-                        exchange(h, dz, dy).wait_send()
-                    exchange(h, dz, dy).wait_recv()
+                    exchange(h, dz, dy).wait()
         for i in range(nz - 1):
             sum_copy(h, i).wait_send()
     for d in range(1, ny):
@@ -742,10 +735,9 @@
             vmem((kv_local * steps, HEAD_DIM, group * QUERY_BLOCK), F32),
             vmem((kv_local, far, tokens, head_cols), BF16),
             vmem((request_count + 1, KEY_BLOCK, wide), BF16),
-            vmem((kv_count, box, wide), BF16),
-            vmem((nz, out_rows, ny * tokens), BF16),
+            vmem((kv_local, kv_count, box, wide), BF16),
+            vmem((nz, ny, out_rows, tokens), BF16),
             vmem((tokens, out_rows), BF16),
-            vmem((max(nz - 1, 1), out_rows, head_cols), F32),
             vmem((kv_local, max(nz - 1, 1), out_rows, head_cols), BF16),
             vmem((kv_local, nz + 1, out_rows, head_cols), BF16),
             dma((3 + nz,)),

time: 259 us -> 248 us (0.958)
  Pallas kernels: 247 us -> 238 us
    pallas_call x1, Pallas kernels: 241 us -> 233 us  [body(): pl.pallas_call(functools.partial(step_kernel, kv_count, tp_count, group,...]
where the time goes in v4:
time: 248 us; the launch traced here: 247 us
  Pallas kernels  238 us (96%)
  local copies, waits for them, and re-layouts  5.98 us (2%)
    pallas_call x1, Pallas kernels, body(): pl.pallas_call(functools.partial(step_kernel, kv_count, tp_count, group,...  233 us
    pallas_call x1, Pallas kernels, body(): pl.pallas_call(functools.partial(settle_kernel, kv_count), grid_spec=pltp...  5.48 us

profile of v4, /device:TPU:0, one launch (start us, length us, event | category | flops | bytes accessed | tf_op | source)
XLA Modules:
  0.0 247.4 jit_solution(6205653559059371198)
XLA Ops:
  0.7 0.8 reshape.178.lists_ref
  1.4 0.0 copy-start.2
  1.5 0.7 fusion.1
  2.2 0.1 select_reduce_fusion.1
  2.3 0.2 convert_reduce_fusion
  2.5 0.6 compare_select_fusion.3
  3.1 0.1 select_reduce_fusion
  3.3 0.0 copy-done.2
  3.3 0.5 broadcast_add_fusion.1.slots_ref
  3.8 0.1 reshape.182
  3.9 0.1 reshape.183
  4.0 0.6 pad.4.wanted_ref
  4.6 0.1 copy.13
  4.7 0.7 add.97.own_ref
  5.3 232.9 %step.1 = (bf16[1024,1024]{1,0:T(8,128)(2,1)}, f32[512,1024]{1,0:T(8,128)}, f32[1024,512]{1,0:T(8,128)}, bf16[2,4096,256]{2,1,0:T(8,128)(2,1)}, bf16[8,32,512]{2...) custom-call(s32[2,128]{1,0:T(2,128)} %copy-done.2, s32[2,128]{1,0:T(2,128)} %get-tuple-element.22.spots_ref, ...), custom_call_target="tpu_custom_call" | custom-call | tf_op jit(solution)/shard_map/step/pallas_call | solution.py:701
  238.3 0.0 copy-start.1
  238.3 5.5 %settle.1 = (bf16[1024,256]{1,0:T(8,128)(2,1)}, bf16[1024,256]{1,0:T(8,128)(2,1)}) custom-call(s32[1]{0:T(128)} %bitcast.3.place_ref, s32[8,128]{1,0:T(8,128)} %bitcast.8, bf16[2,4096,256]{2,1,0:T(8,128)(2,1)} %get-tuple-element.14.got_ref, bf16[8,32,512]{2,1,0:T(8,128)(2,1)} %get-tuple-element.15.pool_ref, f32[1024,512]{1,0:T(8,128)} %get-tuple-element.16.kept_ref), custom_call_target="tpu_custom_call" | custom-call | flops 4194304 | bytes 8388608 | tf_op jit(solution)/shard_map/settle/pallas_call | solution.py:765
  243.8 0.0 copy-done.1
  243.8 0.0 copy-start
  243.8 1.3 copy.17
  245.1 1.0 copy-done
  246.1 1.3 copy.18
  (6 shorter events, 0.0 us)
Async XLA Ops:
  1.4 1.8 copy-start.2
  238.3 5.5 %copy-start.1 = (bf16[1024,1024]{1,0:T(8,128)(2,1)S(1)}, bf16[1024,1024]{1,0:T(8,128)(2,1)}, u32[]{:S(2)}) copy-start(bf16[1024,1024]{1,0:T(8,128)(2,1)} %get-tuple-element.29) | copy-start | bytes 6291460
  243.8 2.3 copy-start
